TPU v7x, 32 devices: a whole 2x2x4 slice. The times are simulated.
32 devices in a mesh: grp: 2 (over y), sp: 4 (over z), tp: 4 (over x, core).
Axes of the slice: x: 2, y: 2, z: 4, core: 2. Of those that a mesh axis runs over, the one named last changes fastest.
Arguments:
- tokens: bfloat16 [1024, 2048], P(('grp', 'sp')), parts along dimension 0, may hold values from -8 to 8
- norm_gain: float32 [2048], replicated, may hold values from 0.1 to 1.9
- w_query: bfloat16 [2048, 1024], P(None, 'tp'), may hold values from -0.125 to 0.125
- w_key: bfloat16 [2048, 1024], P(None, 'tp'), may hold values from -0.125 to 0.125
- w_value: bfloat16 [2048, 1024], P(None, 'tp'), may hold values from -0.125 to 0.125
- w_out: bfloat16 [1024, 2048], P('tp'), may hold values from -0.1875 to 0.1875
- key_rate: bfloat16 [16, 1024], P('tp', ('grp', 'sp')), parts along dimension 1, may hold values from -16 to 1
Outputs:
- layer_out: bfloat16 [1024, 2048], P(('grp', 'sp')), parts along dimension 0
There are 2 independent parts, one for each index of `grp`. A program takes and returns all parts, laid end to end along the dimension named above; an argument that names none is the same for every part. Nothing has to cross between parts.
All inputs are finite; a program needn't handle non-finite values.
Results may differ from a plain program's by a relative error of at most 0.0075.
Values may be sent and summed in bfloat16 or wider, within the bound.
No kernel may reach another device: no remote copies, remote signals or barrier semaphores. Data moves between devices by JAX's collectives and lax.ppermute only.
A program may use at most 64 MiB of HBM per device.

v0:
```python
import functools

import jax
import jax.numpy as jnp
from jax import lax
from jax.experimental import pallas as pl
from jax.experimental.pallas import tpu as pltpu
from jax.sharding import PartitionSpec as P


HD = 64
EPS = 1e-06
F32 = jnp.float32
BF16 = jnp.bfloat16
VMEM_SPEC = pl.BlockSpec(memory_space=pltpu.VMEM)
HBM_SPEC = pl.BlockSpec(memory_space=pltpu.HBM)


def in_hbm(x):
    return pltpu.with_memory_space_constraint(x, pltpu.HBM)


def params(mib):
    return pltpu.CompilerParams(vmem_limit_bytes=mib << 20)


def cost(flops):
    return pl.CostEstimate(flops=flops, bytes_accessed=1 << 20, transcendentals=0)


def project_kernel(chunks, tok_hbm, gain_hbm, rate_hbm, wk_hbm, wv_hbm, wq_hbm, wo_hbm, kv_ref, q_ref, kq_ref, *refs):
    tok, gain, rate, w, normed, sems, w_sems = refs[-7:]
    rows, model = tok.shape
    width = q_ref.shape[1]
    heads = rate.shape[0]
    depth = model // chunks
    small = []
    for i, (src, dst) in enumerate(((tok_hbm, tok), (gain_hbm, gain), (rate_hbm, rate))):
        small.append(pltpu.make_async_copy(src, dst, sems.at[i]))
        small[-1].start()
    copies = []
    for i, ref in enumerate((wk_hbm, wv_hbm, wq_hbm)):
        for c in range(chunks):
            span = pl.ds(c * depth, depth)
            copies.append(pltpu.make_async_copy(ref.at[span], w.at[i, span], w_sems.at[i, c]))
            copies[-1].start()
    tail = None
    if len(refs) > 7:
        span = pl.ds(wo_hbm.shape[0] - refs[0].shape[0], refs[0].shape[0])
        tail = pltpu.make_async_copy(wo_hbm.at[span], refs[0], sems.at[3])
        tail.start()
    for copy in small:
        copy.wait()
    extra = kv_ref.shape[0] - rows
    for ref in (kv_ref, kq_ref):
        ref[pl.ds(rows, extra), :] = jnp.zeros((extra, 2 * width), BF16)
        ref[pl.ds(rows, heads), pl.ds(0, rows)] = rate[...]
    values = tok[...].astype(F32)
    scale = lax.rsqrt(jnp.mean(values * values, axis=-1, keepdims=True) + EPS)
    normed[...] = (values * scale * gain[...]).astype(BF16)
    for i in range(3):
        total = jnp.zeros((rows, width), F32)
        for c in range(chunks):
            span = pl.ds(c * depth, depth)
            copies[i * chunks + c].wait()
            total += jnp.dot(normed[:, span], w[i, span], preferred_element_type=F32)
        out = total.astype(BF16)
        if i < 2:
            kv_ref[pl.ds(0, rows), pl.ds(i * width, width)] = out
        if i == 0:
            kq_ref[pl.ds(0, rows), pl.ds(0, width)] = out
        if i == 2:
            out = out * jnp.asarray(HD**-0.5, BF16)
            q_ref[...] = out
            kq_ref[pl.ds(0, rows), pl.ds(width, width)] = out
    if tail is not None:
        tail.wait()


def project(tokens, gain, rate, w_key, w_value, w_query, w_out, kept):
    rows, model = tokens.shape
    width = w_query.shape[1]
    chunks = 1
    packed = jax.ShapeDtypeStruct((rows + -(-rate.shape[0] // 8) * 8, 2 * width), BF16)
    operands = (tokens, gain.reshape(1, model), rate, w_key, w_value, w_query, w_out)
    brought = (jax.ShapeDtypeStruct((kept, w_out.shape[1]), BF16),) if kept else ()
    return pl.pallas_call(
        functools.partial(project_kernel, chunks),
        out_shape=(packed, jax.ShapeDtypeStruct((rows, width), BF16), packed) + brought,
        in_specs=[HBM_SPEC] * 7,
        out_specs=(VMEM_SPEC,) * (3 + len(brought)),
        scratch_shapes=[
            pltpu.VMEM((rows, model), BF16),
            pltpu.VMEM((1, model), F32),
            pltpu.VMEM(rate.shape, BF16),
            pltpu.VMEM((3, model, width), BF16),
            pltpu.VMEM((rows, model), BF16),
            pltpu.SemaphoreType.DMA((4,)),
            pltpu.SemaphoreType.DMA((3, chunks)),
        ],
        cost_estimate=cost(6 * rows * model * width),
        compiler_params=params(8),
        name="project",
    )(*(in_hbm(x) for x in operands))


def lanes_of(rows, width):
    return lax.broadcasted_iota(jnp.int32, (rows, width), 1) // HD


def stack_heads(q):
    rows, width = q.shape
    lane = lanes_of(rows, width)
    return jnp.concatenate([jnp.where(lane == h, q, jnp.zeros_like(q)) for h in range(width // HD)], axis=0)


def unstack_heads(spread, rows):
    width = spread.shape[1]
    lane = lanes_of(rows, width)
    total = jnp.zeros((rows, width), F32)
    for h in range(width // HD):
        total = total + jnp.where(lane == h, spread[h * rows : (h + 1) * rows], 0.0)
    return total


def later_matrix(rows):
    start = lax.broadcasted_iota(jnp.int32, (2 * rows, 2 * rows), 0) % rows
    stop = lax.broadcasted_iota(jnp.int32, (2 * rows, 2 * rows), 1)
    return ((start > stop) | (stop >= rows)).astype(F32).astype(BF16)


def logs(stacked, packed, later, diagonal):
    rows = later.shape[0] // 2
    width = stacked.shape[1]
    heads = width // HD
    keys = packed[pl.ds(0, rows), pl.ds(0, width)]
    rate = packed[pl.ds(rows, heads), pl.ds(0, rows)].astype(F32)
    scores = lax.dot_general(stacked, keys, (((1,), (1,)), ((), ())), preferred_element_type=F32)
    scores = jnp.concatenate([scores[h * rows : (h + 1) * rows] + rate[h : h + 1] for h in range(heads)], axis=0)
    softened = jnp.log(1.0 + jnp.exp(-jnp.abs(scores)))
    log_keep = jnp.minimum(scores, 0.0) - softened
    log_remain = -jnp.maximum(scores, 0.0) - softened
    mask = None
    if diagonal:
        q_pos = lax.broadcasted_iota(jnp.int32, scores.shape, 0) % rows
        k_pos = lax.broadcasted_iota(jnp.int32, scores.shape, 1)
        mask = k_pos < q_pos
        log_remain = jnp.where(mask, log_remain, 0.0)
    high = log_remain.astype(BF16)
    low = (log_remain - high.astype(F32)).astype(BF16)
    sums = jnp.dot(jnp.concatenate([high, low], axis=1), later, preferred_element_type=F32)
    return log_keep, sums[:, :rows], sums[:, rows:], mask


def absorb(stacked, packed, later, rest, diagonal=False):
    rows = later.shape[0] // 2
    width = stacked.shape[1]
    log_keep, inside, whole, mask = logs(stacked, packed, later, diagonal)
    exponent = log_keep + inside
    if rest is not None:
        exponent = exponent + rest
        whole = whole + rest
    weight = jnp.exp(exponent)
    if diagonal:
        weight = jnp.where(mask, weight, 0.0)
    values = packed[pl.ds(0, rows), pl.ds(width, width)]
    spread = jnp.dot(weight.astype(BF16), values, preferred_element_type=F32)
    return unstack_heads(spread, rows), whole


def own_kernel(q_ref, kv_ref, acc_ref, rest_ref):
    rows = q_ref.shape[0]
    acc_ref[...], rest_ref[...] = absorb(stack_heads(q_ref[...]), kv_ref, later_matrix(rows), None, True)


def ahead_kernel(kq_ref, own_ref, kv_ref, q_ref, acc_ref, rest_ref):
    rows = acc_ref.shape[0]
    width = kq_ref.shape[1] // 2
    here = lax.axis_index("sp") == lax.axis_size("sp") - 2

    @pl.when(here)
    def _():
        q = kq_ref[pl.ds(0, rows), pl.ds(width, width)]
        q_ref[...] = q
        stacked = stack_heads(q)
        later = later_matrix(rows)
        rest = logs(stacked, kq_ref, later, True)[2] + logs(stacked, own_ref, later, False)[2]
        acc_ref[...], rest_ref[...] = absorb(stacked, kv_ref, later, rest)

    @pl.when(jnp.logical_not(here))
    def _():
        for ref in (q_ref, acc_ref, rest_ref):
            ref[...] = jnp.zeros_like(ref)


def more_kernel(sets, last, distance, split, far, kv_ref, *refs):
    ins, outs = refs[: 3 * sets], refs[3 * sets :]
    per = 1 if last else 2
    rows = ins[0].shape[0]
    here = lax.axis_index("sp")
    final = lax.axis_size("sp") - 1
    for i in range(sets):
        takes = here >= distance
        if split and distance > 1:
            takes = jnp.logical_and(takes, here < final)
        if i == 1 or far:
            takes = here == final - 1
        q_ref, acc_ref, rest_ref = ins[3 * i : 3 * i + 3]
        acc_out = outs[per * i]
        rest_out = None if last else outs[per * i + 1]

        @pl.when(takes)
        def _():
            acc, rest = absorb(stack_heads(q_ref[...]), kv_ref, later_matrix(rows), rest_ref[...])
            acc_out[...] = (acc + acc_ref[...]).astype(acc_out.dtype)
            if not last:
                rest_out[...] = rest

        @pl.when(jnp.logical_not(takes))
        def _():
            acc_out[...] = acc_ref[...].astype(acc_out.dtype)
            if not last:
                rest_out[...] = rest_ref[...]


def state_shapes(q, last=False):
    rows, width = q.shape
    if last:
        return (jax.ShapeDtypeStruct((rows, width), BF16),)
    return (
        jax.ShapeDtypeStruct((rows, width), F32),
        jax.ShapeDtypeStruct((width // HD * rows, rows), F32),
    )


def local_call(kernel, flops, out_shape, *operands):
    return pl.pallas_call(
        kernel,
        out_shape=out_shape,
        in_specs=[VMEM_SPEC] * len(operands),
        out_specs=(VMEM_SPEC,) * len(out_shape),
        cost_estimate=cost(flops),
        compiler_params=params(12),
    )(*operands)


def own_block(q, kv):
    return (q, *local_call(own_kernel, 600000000, state_shapes(q), q, kv))


def ahead_blocks(kq, own, kv, q):
    shapes = (jax.ShapeDtypeStruct(q.shape, BF16), *state_shapes(q))
    return local_call(ahead_kernel, 1200000000, shapes, kq, own, kv)


def more_block(kv, states, last, distance, split, far=False):
    q = states[0][0]
    sets = len(states)
    flat = [x for state in states for x in state]
    out = local_call(
        functools.partial(more_kernel, sets, last, distance, split, far), 600000000 * sets, state_shapes(q, last) * sets, kv, *flat
    )
    if last:
        return list(out)
    return [(states[i][0], out[2 * i], out[2 * i + 1]) for i in range(sets)]


def partial_kernel(plan, block, *refs):
    out_ref = refs[-1]
    rows, model = out_ref.shape
    at = 0
    stacks = []
    for has_far, pieces, flips in plan:
        left = refs[at][...]
        at += 1
        if has_far:
            final = lax.axis_index("sp") == lax.axis_size("sp") - 1
            left = left.astype(F32) + jnp.where(final, refs[at][...].astype(F32), 0.0)
            at += 1
        stacks.append((left.astype(BF16), refs[at : at + pieces], flips))
        at += pieces
    for j in range(0, model, block):
        columns = pl.ds(j, block)
        total = jnp.zeros((rows, block), F32)
        for left, pieces, flips in stacks:
            right = [piece[:, columns] for piece in pieces]
            if flips:
                keep = lax.axis_index("grp") == 0
                right[:2] = [jnp.where(keep, right[0], right[1]), jnp.where(keep, right[1], right[0])]
            right = jnp.concatenate(right, axis=0)
            total += jnp.dot(left, right, preferred_element_type=F32)
        out_ref[:, columns] = total.astype(BF16)


def partial_output(stacks):
    plan, flat = [], []
    for near, far, pieces, flips in stacks:
        plan.append((far is not None, len(pieces), flips))
        flat += [near] + ([] if far is None else [far]) + list(pieces)
    rows, depth = stacks[0][0].shape
    model = stacks[0][2][0].shape[1]
    block = 512 if model % 512 == 0 else model
    return pl.pallas_call(
        functools.partial(partial_kernel, tuple(plan), block),
        out_shape=jax.ShapeDtypeStruct((rows, model), BF16),
        in_specs=[VMEM_SPEC] * len(flat),
        out_specs=VMEM_SPEC,
        cost_estimate=cost(2 * rows * model * depth * len(stacks)),
        compiler_params=params(4),
        name="partial",
    )(*flat)


def cut_kernel(w_hbm, first_ref, sem):
    first = first_ref.shape[0]
    at = pl.multiple_of(lax.axis_index("grp") * first, first)
    copy = pltpu.make_async_copy(w_hbm.at[pl.ds(at, first)], first_ref, sem)
    copy.start()
    copy.wait()


def cut(w_out, share):
    return pl.pallas_call(
        cut_kernel,
        out_shape=pltpu.VMEM((share, w_out.shape[1]), BF16),
        in_specs=[HBM_SPEC],
        out_specs=VMEM_SPEC,
        scratch_shapes=[pltpu.SemaphoreType.DMA],
        cost_estimate=cost(1000000),
        compiler_params=params(4),
        name="cut",
    )(in_hbm(w_out))


def tie(x, after):
    return lax.optimization_barrier((x, after))[0]


def layer(tokens, norm_gain, w_query, w_key, w_value, w_out, key_rate):
    shards = lax.axis_size("sp")
    group = lax.axis_size("tp")
    copies = lax.axis_size("grp")
    bits = []
    while 2 << len(bits) <= group:
        bits.append(1 << len(bits))
    bits = bits[::-1]

    def swap(x, bit):
        return lax.ppermute(x, "tp", [(i, i ^ bit) for i in range(group)])

    depth = w_out.shape[0]
    shared = copies == 2 and len(bits) == 2 and depth == 256
    weights = [[w_out]]
    if shared:
        share = depth * 5 // 16
        first = cut(w_out, share)
        first = swap(first, bits[0])
    else:
        for bit in bits[:-1]:
            weights = weights + [[swap(w[0], bit)] for w in weights]

    kept = depth - 2 * share if shared else 0
    kv, q, kq, *half = project(tokens, norm_gain, key_rate, w_key, w_value, w_query, w_out, kept)
    if shared:
        half = swap(half[0], bits[0])
    split = shards > 2
    even = shards % 2 == 0
    behind = range(1, shards - 1 if split else shards)
    arrived = []
    for d in behind:
        stop = behind[-1] + 1
        pairs = [(i, (i + 1) % shards) for i in range(shards)] if d == 1 else [(i, i + d) for i in range(stop - d)]
        arrived.append(lax.ppermute(kv, "sp", pairs))
    if split:
        kq = lax.ppermute(kq, "sp", [(shards - 1, shards - 2)])
    states = [own_block(q, kv)]
    if shared:
        first = tie(first, states[0][1])
        second = lax.ppermute(first, "grp", [(0, 1), (1, 0)])
        weights = weights + [[first, second, half]]
    for i, block in enumerate(arrived):
        last = i == len(arrived) - 1
        if i == 0 and split:
            if last:
                near = more_block(block, states, True, 1, split)
                far = ahead_blocks(kq, kv, block, q)
                states = near + [far[1].astype(BF16)]
            else:
                states = more_block(block, states, False, 1, split)
                kq = tie(kq, states[0][1])
                states = states + [tuple(ahead_blocks(kq, kv, block, q))]
        elif last and len(states) == 2:
            behind_part = more_block(block, states[1:], True, i + 1, split, True)
            states = more_block(block, states[:1], True, i + 1, split) + behind_part
        else:
            states = more_block(block, states, last, i + 1, split)
    if not arrived:
        states = [states[0][1].astype(BF16)]
    near = [states[0]]
    far = [None]

    if split:
        pairs = [(i, i ^ 1) for i in range(shards)] if even else [(shards - 2, shards - 1)]
        far = [lax.ppermute(states[1], "sp", pairs)]
        if len(bits) == 2:
            both = [(a * group + i, b * group + (i ^ bits[0])) for a, b in pairs for i in range(group)]
            far.append(lax.ppermute(states[1], ("sp", "tp"), both))
        else:
            near = [near[0] + jnp.where(lax.axis_index("sp") == shards - 1, far[0], 0)]
            far = [None]
    for bit in bits[:-1]:
        near = near + [swap(x, bit) for x in near]
    far = far + [None] * (len(near) - len(far))
    flips = [shared and i == 1 for i in range(len(near))]
    part = partial_output(list(zip(near, far, weights, flips)))
    if not bits:
        return part
    other = swap(part, bits[-1])
    return (part.astype(F32) + other.astype(F32)).astype(BF16)


def solution(mesh):
    return jax.shard_map(
        layer,
        mesh=mesh,
        in_specs=(
            P(("grp", "sp"), None),
            P(),
            P(None, "tp"),
            P(None, "tp"),
            P(None, "tp"),
            P("tp", None),
            P("tp", ("grp", "sp")),
        ),
        out_specs=P(("grp", "sp"), None),
        check_vma=False,
    )
```

profile of v0, /device:TPU:0, one launch (start us, length us, event | category | flops | bytes accessed | tf_op | source)
XLA Modules:
  0.0 30.4 jit_solution(13410187478325739348)
XLA Ops:
  0.0 1.0 %cut.1 = bf16[80,2048]{1,0:T(8,128)(2,1)S(1)} custom-call(bf16[256,2048]{1,0:T(8,128)(2,1)} %refs_2_.1), custom_call_target="tpu_custom_call" | custom-call | flops 1000000 | bytes 1048576 | tf_op jit(solution)/shard_map/cut/pallas_call | solution.py:323
  1.0 3.0 %collective-permute-start.6 = (bf16[80,2048]{1,0:T(8,128)(2,1)S(1)}, bf16[80,2048]{1,0:T(8,128)(2,1)S(1)}, u32[]{:S(2)}, u32[]{:S(2)}) collective-permute-start(bf16[80,2048]{1,0:T(8,128)(2,1)S(1)} %cut.1), channel_id=1, source_target_pairs={{0,2},{1,3},{2,0},{3,1},{4,6},{5,7},{6,4},{7,5},{8,10},{9,11},{10,... | collective-permute-start | bytes 983048 | tf_op jit(solution)/shard_map/ppermute | solution.py:349
  4.0 2.6 %project.1 = (bf16[136,512]{1,0:T(8,128)(2,1)S(1)}, bf16[128,256]{1,0:T(8,128)(2,1)S(1)}, bf16[136,512]{1,0:T(8,128)(2,1)S(1)}, bf16[96,2048]{1,0:T(8,128)(2,1)S(1)}) custom-call(bf16[128,2048]{1,0:T(8,128)(2,1)} %tok_hbm.1, f32[1,2048]{1,0:T(1,128)} %bitcast.1, bf16[4,128]{1,0:T(4,128)(2,1)} %rate_hbm.1, bf16[2048,256]{1,0:T(8,128)(2,1)} %wk_hbm.1, ...), custom_call_target="tpu_custom_call" | custom-call | flops 402653184 | bytes 1048576 | tf_op jit(solution)/shard_map/project/pallas_call | solution.py:87
  6.7 1.6 %collective-permute-start.1 = (bf16[136,512]{1,0:T(8,128)(2,1)S(1)}, bf16[136,512]{1,0:T(8,128)(2,1)S(1)}, u32[]{:S(2)}, u32[]{:S(2)}) collective-permute-start(bf16[136,512]{1,0:T(8,128)(2,1)S(1)} %get-tuple-element.18.kv_ref.own_ref), channel_id=1, source_target_pairs={{0,4},{4,8},{8,12},{12,0},{1,5},{5,9},{9,13},{13,1},{2,6},{6,10},{... | collective-permute-start | bytes 417800 | tf_op jit(solution)/shard_map/ppermute | solution.py:373
  8.3 0.7 %collective-permute-start.2 = (bf16[136,512]{1,0:T(8,128)(2,1)S(1)}, bf16[136,512]{1,0:T(8,128)(2,1)S(1)}, u32[]{:S(2)}, u32[]{:S(2)}) collective-permute-start(bf16[136,512]{1,0:T(8,128)(2,1)S(1)} %get-tuple-element.24), channel_id=1, source_target_pairs={{12,8},{13,9},{14,10},{15,11},{28,24},{29,25},{30,26},{31,27}} | collective-permute-start | bytes 417800 | tf_op jit(solution)/shard_map/ppermute | solution.py:375
  9.0 5.1 %collective-permute-start = (bf16[136,512]{1,0:T(8,128)(2,1)S(1)}, bf16[136,512]{1,0:T(8,128)(2,1)S(1)}, u32[]{:S(2)}, u32[]{:S(2)}) collective-permute-start(bf16[136,512]{1,0:T(8,128)(2,1)S(1)} %get-tuple-element.18.kv_ref.own_ref), channel_id=1, source_target_pairs={{0,8},{1,9},{2,10},{3,11},{16,24},{17,25},{18,26},{19,27}} | collective-permute-start | bytes 417800 | tf_op jit(solution)/shard_map/ppermute | solution.py:373
  14.1 0.6 %collective-permute-start.8 = (bf16[96,2048]{1,0:T(8,128)(2,1)S(1)}, bf16[96,2048]{1,0:T(8,128)(2,1)S(1)}, u32[]{:S(2)}, u32[]{:S(2)}) collective-permute-start(bf16[96,2048]{1,0:T(8,128)(2,1)S(1)} %get-tuple-element.30), channel_id=1, source_target_pairs={{0,2},{1,3},{2,0},{3,1},{4,6},{5,7},{6,4},{7,5},{8,10},{9,11},{10,... | collective-permute-start | bytes 1179656 | tf_op jit(solution)/shard_map/ppermute | solution.py:349
  14.7 0.6 %shard_map.73 = (f32[128,256]{1,0:T(8,128)S(1)}, f32[512,128]{1,0:T(8,128)S(1)}) custom-call(bf16[128,256]{1,0:T(8,128)(2,1)S(1)} %get-tuple-element.19.q_ref.refs_0_, bf16[136,512]{1,0:T(8,128)(2,1)S(1)} %get-tuple-element.18.kv_ref.own_ref), custom_call_target="tpu_custom_call" | custom-call | flops 600000000 | bytes 1048576 | tf_op jit(solution)/shard_map/pallas_call | solution.py:237
  15.3 0.0 collective-permute-done.6.refs_5_
  15.3 1.6 %collective-permute-start.7 = (bf16[80,2048]{1,0:T(8,128)(2,1)S(1)}, bf16[80,2048]{1,0:T(8,128)(2,1)S(1)}, u32[]{:S(2)}, u32[]{:S(2)}) collective-permute-start(bf16[80,2048]{1,0:T(8,128)(2,1)S(1)} %collective-permute-done.6.refs_5_), channel_id=1, source_target_pairs={{0,16},{16,0},{1,17},{17,1},{2,18},{18,2},{3,19},{19,3},{4,20},{20... | collective-permute-start | bytes 983048 | tf_op jit(solution)/shard_map/ppermute | solution.py:379
  16.9 0.0 collective-permute-done.1.kv_ref
  16.9 0.0 collective-permute-done.2.kq_ref
  17.0 0.4 %collective-permute-done.kv_ref = bf16[136,512]{1,0:T(8,128)(2,1)S(1)} collective-permute-done((bf16[136,512]{1,0:T(8,128)(2,1)S(1)}, bf16[136,512]{1,0:T(8,128)(2,1)S(1)}, u32[]{:S(2)}, u32[]{:S(2)}) %collective-permute-start) | collective-permute-done | bytes 139296 | tf_op jit(solution)/shard_map/ppermute | solution.py:373
  17.4 0.1 collective-permute-start.3
  17.5 0.0 copy-start
  17.5 1.2 %collective-permute-start.4 = (bf16[128,256]{1,0:T(8,128)(2,1)S(1)}, bf16[128,256]{1,0:T(8,128)(2,1)S(1)}, u32[]{:S(2)}, u32[]{:S(2)}) collective-permute-start(bf16[128,256]{1,0:T(8,128)(2,1)S(1)} %shard_map.75.refs_0_), channel_id=1, source_target_pairs={{0,2},{1,3},{2,0},{3,1},{4,6},{5,7},{6,4},{7,5},{8,10},{9,11},{10,... | collective-permute-start | bytes 196616 | tf_op jit(solution)/shard_map/ppermute | solution.py:349
  18.7 2.3 %collective-permute-start.5 = (bf16[128,256]{1,0:T(8,128)(2,1)S(1)}, bf16[128,256]{1,0:T(8,128)(2,1)S(1)}, u32[]{:S(2)}, u32[]{:S(2)}) collective-permute-start(bf16[128,256]{1,0:T(8,128)(2,1)S(1)} %shard_map.77), channel_id=1, source_target_pairs={{0,6},{1,7},{2,4},{3,5},{4,2},{5,3},{6,0},{7,1},{8,14},{9,15},{10,... | collective-permute-start | bytes 196616 | tf_op jit(solution)/shard_map/ppermute | solution.py:407
  21.0 0.7 %collective-permute-done.3.refs_1_ = bf16[128,256]{1,0:T(8,128)(2,1)S(1)} collective-permute-done((bf16[128,256]{1,0:T(8,128)(2,1)S(1)}, bf16[128,256]{1,0:T(8,128)(2,1)S(1)}, u32[]{:S(2)}, u32[]{:S(2)}) %collective-permute-start.3) | collective-permute-done | bytes 65568 | tf_op jit(solution)/shard_map/ppermute | solution.py:404
  21.7 5.3 %collective-permute-done.4.refs_3_ = bf16[128,256]{1,0:T(8,128)(2,1)S(1)} collective-permute-done((bf16[128,256]{1,0:T(8,128)(2,1)S(1)}, bf16[128,256]{1,0:T(8,128)(2,1)S(1)}, u32[]{:S(2)}, u32[]{:S(2)}) %collective-permute-start.4) | collective-permute-done | bytes 65568 | tf_op jit(solution)/shard_map/ppermute | solution.py:349
  27.0 0.0 collective-permute-done.5.refs_4_
  27.0 0.0 collective-permute-done.8.refs_7_
  27.0 0.0 collective-permute-done.7.refs_6_
  27.0 0.0 copy-done
  27.0 0.5 %partial.1 = bf16[128,2048]{1,0:T(8,128)(2,1)S(1)} custom-call(bf16[128,256]{1,0:T(8,128)(2,1)S(1)} %shard_map.75.refs_0_, bf16[128,256]{1,0:T(8,128)(2,1)S(1)} %collective-permute-done.3.refs_1_, bf16[256,2048]{1,0:T(8,128)(2,1)S(1)} %copy-done, bf16[128,256]{1,0:T(8,128)(2,1)S(1)} %collective-permute-done.4.refs_3_, ...), custom_call_target="tpu_custom_call" | custom-call | flops 268435456 | bytes 1048576 | tf_op jit(solution)/shard_map/partial/pallas_call | solution.py:303
  27.5 0.1 collective-permute-start.9
  27.6 1.9 %collective-permute-done.9 = bf16[128,2048]{1,0:T(8,128)(2,1)S(1)} collective-permute-done((bf16[128,2048]{1,0:T(8,128)(2,1)S(1)}, bf16[128,2048]{1,0:T(8,128)(2,1)S(1)}, u32[]{:S(2)}, u32[]{:S(2)}) %collective-permute-start.9) | collective-permute-done | bytes 524320 | tf_op jit(solution)/shard_map/ppermute | solution.py:349
  29.5 0.9 %add_convert_fusion = bf16[128,2048]{1,0:T(8,128)(2,1)} fusion(bf16[128,2048]{1,0:T(8,128)(2,1)S(1)} %collective-permute-done.9, bf16[128,2048]{1,0:T(8,128)(2,1)S(1)} %partial.1), kind=kLoop, calls=%fused_computation | loop fusion | flops 1048576 | bytes 1572864 | tf_op jit(solution)/shard_map/convert_element_type | solution.py:419
  (4 shorter events, 0.1 us)
Async XLA Ops:
  1.0 14.3 %collective-permute-start.6 = (bf16[80,2048]{1,0:T(8,128)(2,1)S(1)}, bf16[80,2048]{1,0:T(8,128)(2,1)S(1)}, u32[]{:S(2)}, u32[]{:S(2)}) collective-permute-start(bf16[80,2048]{1,0:T(8,128)(2,1)S(1)} %cut.1), channel_id=1, source_target_pairs={{0,2},{1,3},{2,0},{3,1},{4,6},{5,7},{6,4},{7,5},{8,10},{9,11},{10,... | collective-permute-start | bytes 983048 | tf_op jit(solution)/shard_map/ppermute | solution.py:349
  6.7 10.2 %collective-permute-start.1 = (bf16[136,512]{1,0:T(8,128)(2,1)S(1)}, bf16[136,512]{1,0:T(8,128)(2,1)S(1)}, u32[]{:S(2)}, u32[]{:S(2)}) collective-permute-start(bf16[136,512]{1,0:T(8,128)(2,1)S(1)} %get-tuple-element.18.kv_ref.own_ref), channel_id=1, source_target_pairs={{0,4},{4,8},{8,12},{12,0},{1,5},{5,9},{9,13},{13,1},{2,6},{6,10},{... | collective-permute-start | bytes 417800 | tf_op jit(solution)/shard_map/ppermute | solution.py:373
  8.3 8.6 %collective-permute-start.2 = (bf16[136,512]{1,0:T(8,128)(2,1)S(1)}, bf16[136,512]{1,0:T(8,128)(2,1)S(1)}, u32[]{:S(2)}, u32[]{:S(2)}) collective-permute-start(bf16[136,512]{1,0:T(8,128)(2,1)S(1)} %get-tuple-element.24), channel_id=1, source_target_pairs={{12,8},{13,9},{14,10},{15,11},{28,24},{29,25},{30,26},{31,27}} | collective-permute-start | bytes 417800 | tf_op jit(solution)/shard_map/ppermute | solution.py:375
  9.0 8.4 %collective-permute-start = (bf16[136,512]{1,0:T(8,128)(2,1)S(1)}, bf16[136,512]{1,0:T(8,128)(2,1)S(1)}, u32[]{:S(2)}, u32[]{:S(2)}) collective-permute-start(bf16[136,512]{1,0:T(8,128)(2,1)S(1)} %get-tuple-element.18.kv_ref.own_ref), channel_id=1, source_target_pairs={{0,8},{1,9},{2,10},{3,11},{16,24},{17,25},{18,26},{19,27}} | collective-permute-start | bytes 417800 | tf_op jit(solution)/shard_map/ppermute | solution.py:373
  14.1 12.9 %collective-permute-start.8 = (bf16[96,2048]{1,0:T(8,128)(2,1)S(1)}, bf16[96,2048]{1,0:T(8,128)(2,1)S(1)}, u32[]{:S(2)}, u32[]{:S(2)}) collective-permute-start(bf16[96,2048]{1,0:T(8,128)(2,1)S(1)} %get-tuple-element.30), channel_id=1, source_target_pairs={{0,2},{1,3},{2,0},{3,1},{4,6},{5,7},{6,4},{7,5},{8,10},{9,11},{10,... | collective-permute-start | bytes 1179656 | tf_op jit(solution)/shard_map/ppermute | solution.py:349
  15.3 11.7 %collective-permute-start.7 = (bf16[80,2048]{1,0:T(8,128)(2,1)S(1)}, bf16[80,2048]{1,0:T(8,128)(2,1)S(1)}, u32[]{:S(2)}, u32[]{:S(2)}) collective-permute-start(bf16[80,2048]{1,0:T(8,128)(2,1)S(1)} %collective-permute-done.6.refs_5_), channel_id=1, source_target_pairs={{0,16},{16,0},{1,17},{17,1},{2,18},{18,2},{3,19},{19,3},{4,20},{20... | collective-permute-start | bytes 983048 | tf_op jit(solution)/shard_map/ppermute | solution.py:379
  17.4 4.3 %collective-permute-start.3 = (bf16[128,256]{1,0:T(8,128)(2,1)S(1)}, bf16[128,256]{1,0:T(8,128)(2,1)S(1)}, u32[]{:S(2)}, u32[]{:S(2)}) collective-permute-start(bf16[128,256]{1,0:T(8,128)(2,1)S(1)} %shard_map.77), channel_id=1, source_target_pairs={{0,4},{4,0},{8,12},{12,8},{1,5},{5,1},{9,13},{13,9},{2,6},{6,2},{1... | collective-permute-start | bytes 196616 | tf_op jit(solution)/shard_map/ppermute | solution.py:404
  17.5 9.5 %copy-start = (bf16[256,2048]{1,0:T(8,128)(2,1)S(1)}, bf16[256,2048]{1,0:T(8,128)(2,1)}, u32[]{:S(2)}) copy-start(bf16[256,2048]{1,0:T(8,128)(2,1)} %refs_2_.1) | copy-start | bytes 3145732
  17.5 9.5 %collective-permute-start.4 = (bf16[128,256]{1,0:T(8,128)(2,1)S(1)}, bf16[128,256]{1,0:T(8,128)(2,1)S(1)}, u32[]{:S(2)}, u32[]{:S(2)}) collective-permute-start(bf16[128,256]{1,0:T(8,128)(2,1)S(1)} %shard_map.75.refs_0_), channel_id=1, source_target_pairs={{0,2},{1,3},{2,0},{3,1},{4,6},{5,7},{6,4},{7,5},{8,10},{9,11},{10,... | collective-permute-start | bytes 196616 | tf_op jit(solution)/shard_map/ppermute | solution.py:349
  18.7 8.3 %collective-permute-start.5 = (bf16[128,256]{1,0:T(8,128)(2,1)S(1)}, bf16[128,256]{1,0:T(8,128)(2,1)S(1)}, u32[]{:S(2)}, u32[]{:S(2)}) collective-permute-start(bf16[128,256]{1,0:T(8,128)(2,1)S(1)} %shard_map.77), channel_id=1, source_target_pairs={{0,6},{1,7},{2,4},{3,5},{4,2},{5,3},{6,0},{7,1},{8,14},{9,15},{10,... | collective-permute-start | bytes 196616 | tf_op jit(solution)/shard_map/ppermute | solution.py:407
  27.5 2.0 %collective-permute-start.9 = (bf16[128,2048]{1,0:T(8,128)(2,1)S(1)}, bf16[128,2048]{1,0:T(8,128)(2,1)S(1)}, u32[]{:S(2)}, u32[]{:S(2)}) collective-permute-start(bf16[128,2048]{1,0:T(8,128)(2,1)S(1)} %partial.1), channel_id=1, source_target_pairs={{0,1},{1,0},{2,3},{3,2},{4,5},{5,4},{6,7},{7,6},{8,9},{9,8},{10,11... | collective-permute-start | bytes 1572872 | tf_op jit(solution)/shard_map/ppermute | solution.py:349
where the time goes:
time: 30.6 us; the launch traced here: 30.4 us
  starting transfers between devices  16.3 us (53%)
  waiting for transfers between devices  8.26 us (27%)
  Pallas kernels  4.8 us (16%)
  other arithmetic  0.92 us (3%)
    ppermute x4, waiting for transfers between devices, swap(): return lax.ppermute(x, 'tp', [(i, i ^ bit) for i in range(group)])  7.18 us
    ppermute x2, starting transfers between devices, layer(): arrived.append(lax.ppermute(kv, 'sp', pairs))  6.75 us
    ppermute x4, starting transfers between devices, swap(): return lax.ppermute(x, 'tp', [(i, i ^ bit) for i in range(group)])  4.92 us
    pallas_call x1, Pallas kernels, project(): pl.pallas_call(functools.partial(project_kernel, chunks), out_shape=(pack...  2.64 us
    ppermute x1, starting transfers between devices, layer(): far.append(lax.ppermute(states[1], ('sp', 'tp'), both))  2.29 us
    ppermute x1, starting transfers between devices, layer(): second = lax.ppermute(first, 'grp', [(0, 1), (1, 0)])  1.58 us
    pallas_call x1, Pallas kernels, cut(): pl.pallas_call(cut_kernel, out_shape=pltpu.VMEM((share, w_out.shape[1]),...  0.98 us
    convert_element_type x1, other arithmetic, layer(): return (part.astype(F32) + other.astype(F32)).astype(BF16)  0.92 us
  transfers between devices with their start and end apart: 10, of which 4 were waited for; matrix products, arithmetic and copies ran while one was open for 0% of the time, Pallas kernels for 11%

commit v1 on v0

--- a/solution.py
+++ b/solution.py
@@ -8,6 +8,7 @@
 from jax.sharding import PartitionSpec as P
 
 
+LOG2E = 1.4426950408889634
 HD = 64
 EPS = 1e-06
 F32 = jnp.float32
@@ -28,7 +29,7 @@
     return pl.CostEstimate(flops=flops, bytes_accessed=1 << 20, transcendentals=0)
 
 
-def project_kernel(chunks, tok_hbm, gain_hbm, rate_hbm, wk_hbm, wv_hbm, wq_hbm, wo_hbm, kv_ref, q_ref, kq_ref, *refs):
+def project_kernel(chunks, tok_hbm, gain_hbm, rate_hbm, wk_hbm, wv_hbm, wq_hbm, wo_hbm, kv_ref, q_ref, *refs):
     tok, gain, rate, w, normed, sems, w_sems = refs[-7:]
     rows, model = tok.shape
     width = q_ref.shape[1]
@@ -52,9 +53,8 @@
     for copy in small:
         copy.wait()
     extra = kv_ref.shape[0] - rows
-    for ref in (kv_ref, kq_ref):
-        ref[pl.ds(rows, extra), :] = jnp.zeros((extra, 2 * width), BF16)
-        ref[pl.ds(rows, heads), pl.ds(0, rows)] = rate[...]
+    kv_ref[pl.ds(rows, extra), :] = jnp.zeros((extra, 2 * width), BF16)
+    kv_ref[pl.ds(rows, heads), pl.ds(0, rows)] = rate[...]
     values = tok[...].astype(F32)
     scale = lax.rsqrt(jnp.mean(values * values, axis=-1, keepdims=True) + EPS)
     normed[...] = (values * scale * gain[...]).astype(BF16)
@@ -67,12 +67,8 @@
         out = total.astype(BF16)
         if i < 2:
             kv_ref[pl.ds(0, rows), pl.ds(i * width, width)] = out
-        if i == 0:
-            kq_ref[pl.ds(0, rows), pl.ds(0, width)] = out
         if i == 2:
-            out = out * jnp.asarray(HD**-0.5, BF16)
-            q_ref[...] = out
-            kq_ref[pl.ds(0, rows), pl.ds(width, width)] = out
+            q_ref[...] = out * jnp.asarray(HD**-0.5, BF16)
     if tail is not None:
         tail.wait()
 
@@ -86,9 +82,9 @@
     brought = (jax.ShapeDtypeStruct((kept, w_out.shape[1]), BF16),) if kept else ()
     return pl.pallas_call(
         functools.partial(project_kernel, chunks),
-        out_shape=(packed, jax.ShapeDtypeStruct((rows, width), BF16), packed) + brought,
+        out_shape=(packed, jax.ShapeDtypeStruct((rows, width), BF16)) + brought,
         in_specs=[HBM_SPEC] * 7,
-        out_specs=(VMEM_SPEC,) * (3 + len(brought)),
+        out_specs=(VMEM_SPEC,) * (2 + len(brought)),
         scratch_shapes=[
             pltpu.VMEM((rows, model), BF16),
             pltpu.VMEM((1, model), F32),
@@ -137,7 +133,8 @@
     rate = packed[pl.ds(rows, heads), pl.ds(0, rows)].astype(F32)
     scores = lax.dot_general(stacked, keys, (((1,), (1,)), ((), ())), preferred_element_type=F32)
     scores = jnp.concatenate([scores[h * rows : (h + 1) * rows] + rate[h : h + 1] for h in range(heads)], axis=0)
-    softened = jnp.log(1.0 + jnp.exp(-jnp.abs(scores)))
+    scores = scores * LOG2E
+    softened = jnp.log2(1.0 + jnp.exp2(-jnp.abs(scores)))
     log_keep = jnp.minimum(scores, 0.0) - softened
     log_remain = -jnp.maximum(scores, 0.0) - softened
     mask = None
@@ -160,7 +157,7 @@
     if rest is not None:
         exponent = exponent + rest
         whole = whole + rest
-    weight = jnp.exp(exponent)
+    weight = jnp.exp2(exponent)
     if diagonal:
         weight = jnp.where(mask, weight, 0.0)
     values = packed[pl.ds(0, rows), pl.ds(width, width)]
@@ -173,24 +170,42 @@
     acc_ref[...], rest_ref[...] = absorb(stack_heads(q_ref[...]), kv_ref, later_matrix(rows), None, True)
 
 
-def ahead_kernel(kq_ref, own_ref, kv_ref, q_ref, acc_ref, rest_ref):
-    rows = acc_ref.shape[0]
-    width = kq_ref.shape[1] // 2
+def ahead_kernel(q_ref, kv_ref, acc_ref, rest_ref):
+    rows = q_ref.shape[0]
     here = lax.axis_index("sp") == lax.axis_size("sp") - 2
 
     @pl.when(here)
     def _():
-        q = kq_ref[pl.ds(0, rows), pl.ds(width, width)]
-        q_ref[...] = q
-        stacked = stack_heads(q)
-        later = later_matrix(rows)
-        rest = logs(stacked, kq_ref, later, True)[2] + logs(stacked, own_ref, later, False)[2]
-        acc_ref[...], rest_ref[...] = absorb(stacked, kv_ref, later, rest)
+        acc_ref[...], rest_ref[...] = absorb(stack_heads(q_ref[...]), kv_ref, later_matrix(rows), None)
 
     @pl.when(jnp.logical_not(here))
     def _():
-        for ref in (q_ref, acc_ref, rest_ref):
+        for ref in (acc_ref, rest_ref):
             ref[...] = jnp.zeros_like(ref)
+
+
+def far_factor(rest, rows, heads):
+    lines = [jnp.transpose(rest[h * rows : (h + 1) * rows])[:1] for h in range(heads)]
+    return jnp.exp2(jnp.concatenate(lines, axis=0)).astype(BF16)
+
+
+def add_far(near_ref, far_ref, out_ref):
+    rows, width = far_ref.shape
+    heads = width // HD
+    final = lax.axis_index("sp") == lax.axis_size("sp") - 1
+
+    @pl.when(jnp.logical_not(final))
+    def _():
+        out_ref[...] = near_ref[pl.ds(0, rows), :]
+
+    @pl.when(final)
+    def _():
+        factor = near_ref[pl.ds(rows, heads), pl.ds(0, rows)]
+        lane = lax.broadcasted_iota(jnp.int32, (heads, width), 1) // HD
+        pick = (lane == lax.broadcasted_iota(jnp.int32, (heads, width), 0)).astype(F32).astype(BF16)
+        wide = lax.dot_general(factor, pick, (((0,), (0,)), ((), ())), preferred_element_type=F32)
+        total = near_ref[pl.ds(0, rows), :].astype(F32) + far_ref[...].astype(F32) * wide
+        out_ref[...] = total.astype(BF16)
 
 
 def more_kernel(sets, last, distance, split, far, kv_ref, *refs):
@@ -208,17 +223,23 @@
         q_ref, acc_ref, rest_ref = ins[3 * i : 3 * i + 3]
         acc_out = outs[per * i]
         rest_out = None if last else outs[per * i + 1]
+        heads = acc_ref.shape[1] // HD
+        tails = last and split and i == 0 and not far
 
         @pl.when(takes)
         def _():
             acc, rest = absorb(stack_heads(q_ref[...]), kv_ref, later_matrix(rows), rest_ref[...])
-            acc_out[...] = (acc + acc_ref[...]).astype(acc_out.dtype)
+            acc_out[pl.ds(0, rows), :] = (acc + acc_ref[...]).astype(acc_out.dtype)
+            if tails:
+                acc_out[pl.ds(rows, heads), pl.ds(0, rows)] = far_factor(rest, rows, heads)
             if not last:
                 rest_out[...] = rest
 
         @pl.when(jnp.logical_not(takes))
         def _():
-            acc_out[...] = acc_ref[...].astype(acc_out.dtype)
+            acc_out[pl.ds(0, rows), :] = acc_ref[...].astype(acc_out.dtype)
+            if tails:
+                acc_out[pl.ds(rows, heads), pl.ds(0, rows)] = far_factor(rest_ref[...], rows, heads)
             if not last:
                 rest_out[...] = rest_ref[...]
 
@@ -248,36 +269,43 @@
     return (q, *local_call(own_kernel, 600000000, state_shapes(q), q, kv))
 
 
-def ahead_blocks(kq, own, kv, q):
-    shapes = (jax.ShapeDtypeStruct(q.shape, BF16), *state_shapes(q))
-    return local_call(ahead_kernel, 1200000000, shapes, kq, own, kv)
+def ahead_blocks(q, kv):
+    return (q, *local_call(ahead_kernel, 600000000, state_shapes(q), q, kv))
 
 
 def more_block(kv, states, last, distance, split, far=False):
     q = states[0][0]
     sets = len(states)
     flat = [x for state in states for x in state]
-    out = local_call(
-        functools.partial(more_kernel, sets, last, distance, split, far), 600000000 * sets, state_shapes(q, last) * sets, kv, *flat
-    )
+    shapes = state_shapes(q, last) * sets
+    if last and split and not far:
+        rows, width = q.shape
+        shapes = (jax.ShapeDtypeStruct((rows + -(-(width // HD) // 8) * 8, width), BF16), *shapes[1:])
+    kernel = functools.partial(more_kernel, sets, last, distance, split, far)
+    out = local_call(kernel, 600000000 * sets, shapes, kv, *flat)
     if last:
         return list(out)
     return [(states[i][0], out[2 * i], out[2 * i + 1]) for i in range(sets)]
 
 
+def merge(near, far):
+    return local_call(add_far, 1000000, (jax.ShapeDtypeStruct(far.shape, BF16),), near, far)[0]
+
+
 def partial_kernel(plan, block, *refs):
-    out_ref = refs[-1]
+    out_ref, merged = refs[-2:]
     rows, model = out_ref.shape
     at = 0
     stacks = []
     for has_far, pieces, flips in plan:
-        left = refs[at][...]
-        at += 1
         if has_far:
-            final = lax.axis_index("sp") == lax.axis_size("sp") - 1
-            left = left.astype(F32) + jnp.where(final, refs[at][...].astype(F32), 0.0)
+            add_far(refs[at], refs[at + 1], merged)
+            left = merged[...]
+            at += 2
+        else:
+            left = refs[at][...]
             at += 1
-        stacks.append((left.astype(BF16), refs[at : at + pieces], flips))
+        stacks.append((left, refs[at : at + pieces], flips))
         at += pieces
     for j in range(0, model, block):
         columns = pl.ds(j, block)
@@ -297,7 +325,7 @@
     for near, far, pieces, flips in stacks:
         plan.append((far is not None, len(pieces), flips))
         flat += [near] + ([] if far is None else [far]) + list(pieces)
-    rows, depth = stacks[0][0].shape
+    rows, depth = (stacks[0][0] if stacks[0][1] is None else stacks[0][1]).shape
     model = stacks[0][2][0].shape[1]
     block = 512 if model % 512 == 0 else model
     return pl.pallas_call(
@@ -305,10 +333,37 @@
         out_shape=jax.ShapeDtypeStruct((rows, model), BF16),
         in_specs=[VMEM_SPEC] * len(flat),
         out_specs=VMEM_SPEC,
+        scratch_shapes=[pltpu.VMEM((rows, depth), BF16)],
         cost_estimate=cost(2 * rows * model * depth * len(stacks)),
         compiler_params=params(4),
         name="partial",
     )(*flat)
+
+
+def finish_kernel(span, mine_ref, theirs_ref, out_hbm, staged, sems):
+    copies = []
+    for i in range(staged.shape[0] // span):
+        run = pl.ds(i * span, span)
+        staged[run, :] = (mine_ref[run, :].astype(F32) + theirs_ref[run, :].astype(F32)).astype(BF16)
+        copies.append(pltpu.make_async_copy(staged.at[run], out_hbm.at[run], sems.at[i]))
+        copies[-1].start()
+    for copy in copies:
+        copy.wait()
+
+
+def finish(mine, theirs):
+    rows, model = mine.shape
+    span = 32 if rows % 32 == 0 else rows
+    return pl.pallas_call(
+        functools.partial(finish_kernel, span),
+        out_shape=jax.ShapeDtypeStruct((rows, model), BF16),
+        in_specs=[VMEM_SPEC] * 2,
+        out_specs=HBM_SPEC,
+        scratch_shapes=[pltpu.VMEM((rows, model), BF16), pltpu.SemaphoreType.DMA((rows // span,))],
+        cost_estimate=cost(1000000),
+        compiler_params=params(4),
+        name="finish",
+    )(mine, theirs)
 
 
 def cut_kernel(w_hbm, first_ref, sem):
@@ -360,10 +415,10 @@
             weights = weights + [[swap(w[0], bit)] for w in weights]
 
     kept = depth - 2 * share if shared else 0
-    kv, q, kq, *half = project(tokens, norm_gain, key_rate, w_key, w_value, w_query, w_out, kept)
+    kv, q, *half = project(tokens, norm_gain, key_rate, w_key, w_value, w_query, w_out, kept)
     if shared:
         half = swap(half[0], bits[0])
-    split = shards > 2
+    split = shards > 2 and w_query.shape[1] >= tokens.shape[0]
     even = shards % 2 == 0
     behind = range(1, shards - 1 if split else shards)
     arrived = []
@@ -372,7 +427,7 @@
         pairs = [(i, (i + 1) % shards) for i in range(shards)] if d == 1 else [(i, i + d) for i in range(stop - d)]
         arrived.append(lax.ppermute(kv, "sp", pairs))
     if split:
-        kq = lax.ppermute(kq, "sp", [(shards - 1, shards - 2)])
+        last_q = lax.ppermute(q, "sp", [(shards - 1, shards - 2)])
     states = [own_block(q, kv)]
     if shared:
         first = tie(first, states[0][1])
@@ -383,12 +438,12 @@
         if i == 0 and split:
             if last:
                 near = more_block(block, states, True, 1, split)
-                far = ahead_blocks(kq, kv, block, q)
+                far = ahead_blocks(last_q, block)
                 states = near + [far[1].astype(BF16)]
             else:
                 states = more_block(block, states, False, 1, split)
-                kq = tie(kq, states[0][1])
-                states = states + [tuple(ahead_blocks(kq, kv, block, q))]
+                last_q = tie(last_q, states[0][1])
+                states = states + [ahead_blocks(last_q, block)]
         elif last and len(states) == 2:
             behind_part = more_block(block, states[1:], True, i + 1, split, True)
             states = more_block(block, states[:1], True, i + 1, split) + behind_part
@@ -406,17 +461,19 @@
             both = [(a * group + i, b * group + (i ^ bits[0])) for a, b in pairs for i in range(group)]
             far.append(lax.ppermute(states[1], ("sp", "tp"), both))
         else:
-            near = [near[0] + jnp.where(lax.axis_index("sp") == shards - 1, far[0], 0)]
+            near = [merge(near[0], far[0])]
             far = [None]
     for bit in bits[:-1]:
         near = near + [swap(x, bit) for x in near]
+    if len(far) == 2:
+        near[1], far[1] = merge(near[1], far[1]), None
     far = far + [None] * (len(near) - len(far))
     flips = [shared and i == 1 for i in range(len(near))]
     part = partial_output(list(zip(near, far, weights, flips)))
     if not bits:
         return part
     other = swap(part, bits[-1])
-    return (part.astype(F32) + other.astype(F32)).astype(BF16)
+    return finish(part, other)
 
 
 def solution(mesh):

time: 30.6 us -> 31.7 us (1.036)
  the two profiles are of different devices: /device:TPU:0 before, /device:TPU:25 now
where the time goes in v1:
time: 31.7 us; the launch traced here: 31.2 us
  starting transfers between devices  16.3 us (51%)
  waiting for transfers between devices  8.16 us (26%)
  Pallas kernels  6.66 us (21%)
    ppermute x4, starting transfers between devices, swap(): return lax.ppermute(x, 'tp', [(i, i ^ bit) for i in range(group)])  8.42 us
    ppermute x4, waiting for transfers between devices, swap(): return lax.ppermute(x, 'tp', [(i, i ^ bit) for i in range(group)])  4.63 us
    ppermute x1, starting transfers between devices, layer(): far.append(lax.ppermute(states[1], ('sp', 'tp'), both))  3.72 us
    pallas_call x1, Pallas kernels, project(): pl.pallas_call(functools.partial(project_kernel, chunks), out_shape=(pack...  2.64 us
    ppermute x1, starting transfers between devices, layer(): last_q = lax.ppermute(q, 'sp', [(shards - 1, shards - 2)])  2.06 us
    ppermute x1, waiting for transfers between devices, layer(): far.append(lax.ppermute(states[1], ('sp', 'tp'), both))  1.55 us
    pallas_call x6, Pallas kernels, local_call(): pl.pallas_call(kernel, out_shape=out_shape, in_specs=[VMEM_SPEC] * len(op...  1.51 us
    ppermute x1, waiting for transfers between devices, layer(): far = [lax.ppermute(states[1], 'sp', pairs)]  1.26 us
  transfers between devices with their start and end apart: 10, of which 5 were waited for; matrix products, arithmetic and copies ran while one was open for 0% of the time, Pallas kernels for 13%

profile of v1, /device:TPU:25, one launch (start us, length us, event | category | flops | bytes accessed | tf_op | source)
XLA Modules:
  0.0 31.2 jit_solution(9878234250851659042)
XLA Ops:
  0.0 1.0 %cut.1 = bf16[80,2048]{1,0:T(8,128)(2,1)S(1)} custom-call(bf16[256,2048]{1,0:T(8,128)(2,1)} %refs_2_.1), custom_call_target="tpu_custom_call" | custom-call | flops 1000000 | bytes 1048576 | tf_op jit(solution)/shard_map/cut/pallas_call | solution.py:378
  1.0 1.3 %collective-permute-start.6 = (bf16[80,2048]{1,0:T(8,128)(2,1)S(1)}, bf16[80,2048]{1,0:T(8,128)(2,1)S(1)}, u32[]{:S(2)}, u32[]{:S(2)}) collective-permute-start(bf16[80,2048]{1,0:T(8,128)(2,1)S(1)} %cut.1), channel_id=1, source_target_pairs={{0,2},{1,3},{2,0},{3,1},{4,6},{5,7},{6,4},{7,5},{8,10},{9,11},{10,... | collective-permute-start | bytes 983048 | tf_op jit(solution)/shard_map/ppermute | solution.py:404
  2.3 2.6 %project.1 = (bf16[136,512]{1,0:T(8,128)(2,1)S(1)}, bf16[128,256]{1,0:T(8,128)(2,1)S(1)}, bf16[96,2048]{1,0:T(8,128)(2,1)S(1)}) custom-call(bf16[128,2048]{1,0:T(8,128)(2,1)} %tok_hbm.1, f32[1,2048]{1,0:T(1,128)} %bitcast.1, bf16[4,128]{1,0:T(4,128)(2,1)} %rate_hbm.1, bf16[2048,256]{1,0:T(8,128)(2,1)} %wk_hbm.1, bf16[2048,256]{1,0:T(8,128)(2,1)} %wv_hbm.1, ...), custom_call_target="tpu_custom_call" | custom-call | flops 402653184 | bytes 1048576 | tf_op jit(solution)/shard_map/project/pallas_call | solution.py:83
  4.9 0.1 collective-permute-start.1
  5.0 0.3 %collective-permute-start.8 = (bf16[96,2048]{1,0:T(8,128)(2,1)S(1)}, bf16[96,2048]{1,0:T(8,128)(2,1)S(1)}, u32[]{:S(2)}, u32[]{:S(2)}) collective-permute-start(bf16[96,2048]{1,0:T(8,128)(2,1)S(1)} %get-tuple-element.26), channel_id=1, source_target_pairs={{0,2},{1,3},{2,0},{3,1},{4,6},{5,7},{6,4},{7,5},{8,10},{9,11},{10,... | collective-permute-start | bytes 1179656 | tf_op jit(solution)/shard_map/ppermute | solution.py:404
  5.3 0.7 %collective-permute-start = (bf16[136,512]{1,0:T(8,128)(2,1)S(1)}, bf16[136,512]{1,0:T(8,128)(2,1)S(1)}, u32[]{:S(2)}, u32[]{:S(2)}) collective-permute-start(bf16[136,512]{1,0:T(8,128)(2,1)S(1)} %get-tuple-element.16.kv_ref), channel_id=1, source_target_pairs={{0,8},{1,9},{2,10},{3,11},{16,24},{17,25},{18,26},{19,27}} | collective-permute-start | bytes 417800 | tf_op jit(solution)/shard_map/ppermute | solution.py:428
  6.0 0.6 %shard_map.73 = (f32[128,256]{1,0:T(8,128)S(1)}, f32[512,128]{1,0:T(8,128)S(1)}) custom-call(bf16[128,256]{1,0:T(8,128)(2,1)S(1)} %get-tuple-element.17.q_ref.refs_0_, bf16[136,512]{1,0:T(8,128)(2,1)S(1)} %get-tuple-element.16.kv_ref), custom_call_target="tpu_custom_call" | custom-call | flops 600000000 | bytes 1048576 | tf_op jit(solution)/shard_map/pallas_call | solution.py:258
  6.6 3.1 %collective-permute-done.6.refs_4_ = bf16[80,2048]{1,0:T(8,128)(2,1)S(1)} collective-permute-done((bf16[80,2048]{1,0:T(8,128)(2,1)S(1)}, bf16[80,2048]{1,0:T(8,128)(2,1)S(1)}, u32[]{:S(2)}, u32[]{:S(2)}) %collective-permute-start.6) | collective-permute-done | bytes 327712 | tf_op jit(solution)/shard_map/ppermute | solution.py:404
  9.6 1.2 %collective-permute-start.7 = (bf16[80,2048]{1,0:T(8,128)(2,1)S(1)}, bf16[80,2048]{1,0:T(8,128)(2,1)S(1)}, u32[]{:S(2)}, u32[]{:S(2)}) collective-permute-start(bf16[80,2048]{1,0:T(8,128)(2,1)S(1)} %collective-permute-done.6.refs_4_), channel_id=1, source_target_pairs={{0,16},{16,0},{1,17},{17,1},{2,18},{18,2},{3,19},{19,3},{4,20},{20... | collective-permute-start | bytes 983048 | tf_op jit(solution)/shard_map/ppermute | solution.py:434
  10.9 2.1 %collective-permute-start.2 = (bf16[128,256]{1,0:T(8,128)(2,1)S(1)}, bf16[128,256]{1,0:T(8,128)(2,1)S(1)}, u32[]{:S(2)}, u32[]{:S(2)}) collective-permute-start(bf16[128,256]{1,0:T(8,128)(2,1)S(1)} %get-tuple-element.17.q_ref.refs_0_), channel_id=1, source_target_pairs={{12,8},{13,9},{14,10},{15,11},{28,24},{29,25},{30,26},{31,27}} | collective-permute-start | bytes 196616 | tf_op jit(solution)/shard_map/ppermute | solution.py:430
  13.0 0.0 collective-permute-done.1.kv_ref
  13.0 0.6 %shard_map.74 = (f32[128,256]{1,0:T(8,128)S(1)}, f32[512,128]{1,0:T(8,128)S(1)}) custom-call(bf16[136,512]{1,0:T(8,128)(2,1)S(1)} %collective-permute-done.1.kv_ref, bf16[128,256]{1,0:T(8,128)(2,1)S(1)} %get-tuple-element.17.q_ref.refs_0_, f32[128,256]{1,0:T(8,128)S(1)} %get-tuple-element.18.refs_1_, f32[512,128]{1,0:T(8,128)S(1)} %get-tuple-element.19.refs_2_), custom_call_target="tpu_custom_call" | custom-call | flops 600000000 | bytes 1048576 | tf_op jit(solution)/shard_map/pallas_call | solution.py:258
  13.6 0.7 %collective-permute-done.2.q_ref.refs_0_ = bf16[128,256]{1,0:T(8,128)(2,1)S(1)} collective-permute-done((bf16[128,256]{1,0:T(8,128)(2,1)S(1)}, bf16[128,256]{1,0:T(8,128)(2,1)S(1)}, u32[]{:S(2)}, u32[]{:S(2)}) %collective-permute-start.2) | collective-permute-done | bytes 65568 | tf_op jit(solution)/shard_map/ppermute | solution.py:430
  14.3 0.0 collective-permute-done.kv_ref
  14.3 0.1 shard_map.75.refs_0_
  14.4 1.3 %collective-permute-start.4 = (bf16[136,256]{1,0:T(8,128)(2,1)S(1)}, bf16[136,256]{1,0:T(8,128)(2,1)S(1)}, u32[]{:S(2)}, u32[]{:S(2)}) collective-permute-start(bf16[136,256]{1,0:T(8,128)(2,1)S(1)} %shard_map.75.refs_0_), channel_id=1, source_target_pairs={{0,2},{1,3},{2,0},{3,1},{4,6},{5,7},{6,4},{7,5},{8,10},{9,11},{10,... | collective-permute-start | bytes 208904 | tf_op jit(solution)/shard_map/ppermute | solution.py:404
  15.7 0.0 copy-start
  15.7 3.7 %collective-permute-start.5 = (bf16[128,256]{1,0:T(8,128)(2,1)S(1)}, bf16[128,256]{1,0:T(8,128)(2,1)S(1)}, u32[]{:S(2)}, u32[]{:S(2)}) collective-permute-start(bf16[128,256]{1,0:T(8,128)(2,1)S(1)} %shard_map.77), channel_id=1, source_target_pairs={{0,6},{1,7},{2,4},{3,5},{4,2},{5,3},{6,0},{7,1},{8,14},{9,15},{10,... | collective-permute-start | bytes 196616 | tf_op jit(solution)/shard_map/ppermute | solution.py:462
  19.4 0.1 collective-permute-start.3
  19.5 1.5 %collective-permute-done.5.far_ref = bf16[128,256]{1,0:T(8,128)(2,1)S(1)} collective-permute-done((bf16[128,256]{1,0:T(8,128)(2,1)S(1)}, bf16[128,256]{1,0:T(8,128)(2,1)S(1)}, u32[]{:S(2)}, u32[]{:S(2)}) %collective-permute-start.5) | collective-permute-done | bytes 65568 | tf_op jit(solution)/shard_map/ppermute | solution.py:462
  21.1 0.0 collective-permute-done.4.near_ref
  21.1 0.2 shard_map.78.refs_3_
  21.3 1.3 %collective-permute-done.3.refs_1_ = bf16[128,256]{1,0:T(8,128)(2,1)S(1)} collective-permute-done((bf16[128,256]{1,0:T(8,128)(2,1)S(1)}, bf16[128,256]{1,0:T(8,128)(2,1)S(1)}, u32[]{:S(2)}, u32[]{:S(2)}) %collective-permute-start.3) | collective-permute-done | bytes 65568 | tf_op jit(solution)/shard_map/ppermute | solution.py:459
  22.5 0.0 collective-permute-done.8.refs_6_
  22.5 0.0 collective-permute-done.7.refs_5_
  22.5 0.0 copy-done
  22.6 0.7 %partial.1.mine_ref = bf16[128,2048]{1,0:T(8,128)(2,1)S(1)} custom-call(bf16[136,256]{1,0:T(8,128)(2,1)S(1)} %shard_map.75.refs_0_, bf16[128,256]{1,0:T(8,128)(2,1)S(1)} %collective-permute-done.3.refs_1_, bf16[256,2048]{1,0:T(8,128)(2,1)S(1)} %copy-done, bf16[128,256]{1,0:T(8,128)(2,1)S(1)} %shard_map.78.refs_3_, ...), custom_call_target="tpu_custom_call" | custom-call | flops 268435456 | bytes 1048576 | tf_op jit(solution)/shard_map/partial/pallas_call | solution.py:331
  23.2 5.6 %collective-permute-start.9 = (bf16[128,2048]{1,0:T(8,128)(2,1)S(1)}, bf16[128,2048]{1,0:T(8,128)(2,1)S(1)}, u32[]{:S(2)}, u32[]{:S(2)}) collective-permute-start(bf16[128,2048]{1,0:T(8,128)(2,1)S(1)} %partial.1.mine_ref), channel_id=1, source_target_pairs={{0,1},{1,0},{2,3},{3,2},{4,5},{5,4},{6,7},{7,6},{8,9},{9,8},{10,11... | collective-permute-start | bytes 1572872 | tf_op jit(solution)/shard_map/ppermute | solution.py:404
  28.8 1.5 %collective-permute-done.9.theirs_ref = bf16[128,2048]{1,0:T(8,128)(2,1)S(1)} collective-permute-done((bf16[128,2048]{1,0:T(8,128)(2,1)S(1)}, bf16[128,2048]{1,0:T(8,128)(2,1)S(1)}, u32[]{:S(2)}, u32[]{:S(2)}) %collective-permute-start.9) | collective-permute-done | bytes 524320 | tf_op jit(solution)/shard_map/ppermute | solution.py:404
  30.3 0.8 %finish.1 = bf16[128,2048]{1,0:T(8,128)(2,1)} custom-call(bf16[128,2048]{1,0:T(8,128)(2,1)S(1)} %partial.1.mine_ref, bf16[128,2048]{1,0:T(8,128)(2,1)S(1)} %collective-permute-done.9.theirs_ref), custom_call_target="tpu_custom_call" | custom-call | flops 1000000 | bytes 1048576 | tf_op jit(solution)/shard_map/finish/pallas_call | solution.py:357
  (2 shorter events, 0.1 us)
Async XLA Ops:
  1.0 8.7 %collective-permute-start.6 = (bf16[80,2048]{1,0:T(8,128)(2,1)S(1)}, bf16[80,2048]{1,0:T(8,128)(2,1)S(1)}, u32[]{:S(2)}, u32[]{:S(2)}) collective-permute-start(bf16[80,2048]{1,0:T(8,128)(2,1)S(1)} %cut.1), channel_id=1, source_target_pairs={{0,2},{1,3},{2,0},{3,1},{4,6},{5,7},{6,4},{7,5},{8,10},{9,11},{10,... | collective-permute-start | bytes 983048 | tf_op jit(solution)/shard_map/ppermute | solution.py:404
  4.9 8.1 %collective-permute-start.1 = (bf16[136,512]{1,0:T(8,128)(2,1)S(1)}, bf16[136,512]{1,0:T(8,128)(2,1)S(1)}, u32[]{:S(2)}, u32[]{:S(2)}) collective-permute-start(bf16[136,512]{1,0:T(8,128)(2,1)S(1)} %get-tuple-element.16.kv_ref), channel_id=1, source_target_pairs={{0,4},{4,8},{8,12},{12,0},{1,5},{5,9},{9,13},{13,1},{2,6},{6,10},{... | collective-permute-start | bytes 417800 | tf_op jit(solution)/shard_map/ppermute | solution.py:428
  5.0 17.6 %collective-permute-start.8 = (bf16[96,2048]{1,0:T(8,128)(2,1)S(1)}, bf16[96,2048]{1,0:T(8,128)(2,1)S(1)}, u32[]{:S(2)}, u32[]{:S(2)}) collective-permute-start(bf16[96,2048]{1,0:T(8,128)(2,1)S(1)} %get-tuple-element.26), channel_id=1, source_target_pairs={{0,2},{1,3},{2,0},{3,1},{4,6},{5,7},{6,4},{7,5},{8,10},{9,11},{10,... | collective-permute-start | bytes 1179656 | tf_op jit(solution)/shard_map/ppermute | solution.py:404
  5.3 9.0 %collective-permute-start = (bf16[136,512]{1,0:T(8,128)(2,1)S(1)}, bf16[136,512]{1,0:T(8,128)(2,1)S(1)}, u32[]{:S(2)}, u32[]{:S(2)}) collective-permute-start(bf16[136,512]{1,0:T(8,128)(2,1)S(1)} %get-tuple-element.16.kv_ref), channel_id=1, source_target_pairs={{0,8},{1,9},{2,10},{3,11},{16,24},{17,25},{18,26},{19,27}} | collective-permute-start | bytes 417800 | tf_op jit(solution)/shard_map/ppermute | solution.py:428
  9.6 12.9 %collective-permute-start.7 = (bf16[80,2048]{1,0:T(8,128)(2,1)S(1)}, bf16[80,2048]{1,0:T(8,128)(2,1)S(1)}, u32[]{:S(2)}, u32[]{:S(2)}) collective-permute-start(bf16[80,2048]{1,0:T(8,128)(2,1)S(1)} %collective-permute-done.6.refs_4_), channel_id=1, source_target_pairs={{0,16},{16,0},{1,17},{17,1},{2,18},{18,2},{3,19},{19,3},{4,20},{20... | collective-permute-start | bytes 983048 | tf_op jit(solution)/shard_map/ppermute | solution.py:434
  10.9 3.4 %collective-permute-start.2 = (bf16[128,256]{1,0:T(8,128)(2,1)S(1)}, bf16[128,256]{1,0:T(8,128)(2,1)S(1)}, u32[]{:S(2)}, u32[]{:S(2)}) collective-permute-start(bf16[128,256]{1,0:T(8,128)(2,1)S(1)} %get-tuple-element.17.q_ref.refs_0_), channel_id=1, source_target_pairs={{12,8},{13,9},{14,10},{15,11},{28,24},{29,25},{30,26},{31,27}} | collective-permute-start | bytes 196616 | tf_op jit(solution)/shard_map/ppermute | solution.py:430
  14.4 6.7 %collective-permute-start.4 = (bf16[136,256]{1,0:T(8,128)(2,1)S(1)}, bf16[136,256]{1,0:T(8,128)(2,1)S(1)}, u32[]{:S(2)}, u32[]{:S(2)}) collective-permute-start(bf16[136,256]{1,0:T(8,128)(2,1)S(1)} %shard_map.75.refs_0_), channel_id=1, source_target_pairs={{0,2},{1,3},{2,0},{3,1},{4,6},{5,7},{6,4},{7,5},{8,10},{9,11},{10,... | collective-permute-start | bytes 208904 | tf_op jit(solution)/shard_map/ppermute | solution.py:404
  15.7 6.9 %copy-start = (bf16[256,2048]{1,0:T(8,128)(2,1)S(1)}, bf16[256,2048]{1,0:T(8,128)(2,1)}, u32[]{:S(2)}) copy-start(bf16[256,2048]{1,0:T(8,128)(2,1)} %refs_2_.1) | copy-start | bytes 3145732
  15.7 5.4 %collective-permute-start.5 = (bf16[128,256]{1,0:T(8,128)(2,1)S(1)}, bf16[128,256]{1,0:T(8,128)(2,1)S(1)}, u32[]{:S(2)}, u32[]{:S(2)}) collective-permute-start(bf16[128,256]{1,0:T(8,128)(2,1)S(1)} %shard_map.77), channel_id=1, source_target_pairs={{0,6},{1,7},{2,4},{3,5},{4,2},{5,3},{6,0},{7,1},{8,14},{9,15},{10,... | collective-permute-start | bytes 196616 | tf_op jit(solution)/shard_map/ppermute | solution.py:462
  19.4 3.1 %collective-permute-start.3 = (bf16[128,256]{1,0:T(8,128)(2,1)S(1)}, bf16[128,256]{1,0:T(8,128)(2,1)S(1)}, u32[]{:S(2)}, u32[]{:S(2)}) collective-permute-start(bf16[128,256]{1,0:T(8,128)(2,1)S(1)} %shard_map.77), channel_id=1, source_target_pairs={{0,4},{4,0},{8,12},{12,8},{1,5},{5,1},{9,13},{13,9},{2,6},{6,2},{1... | collective-permute-start | bytes 196616 | tf_op jit(solution)/shard_map/ppermute | solution.py:459
  23.2 7.1 %collective-permute-start.9 = (bf16[128,2048]{1,0:T(8,128)(2,1)S(1)}, bf16[128,2048]{1,0:T(8,128)(2,1)S(1)}, u32[]{:S(2)}, u32[]{:S(2)}) collective-permute-start(bf16[128,2048]{1,0:T(8,128)(2,1)S(1)} %partial.1.mine_ref), channel_id=1, source_target_pairs={{0,1},{1,0},{2,3},{3,2},{4,5},{5,4},{6,7},{7,6},{8,9},{9,8},{10,11... | collective-permute-start | bytes 1572872 | tf_op jit(solution)/shard_map/ppermute | solution.py:404

commit v2 on v1

--- a/solution.py
+++ b/solution.py
@@ -8,6 +8,7 @@
 from jax.sharding import PartitionSpec as P
 
 
+LATE_BLOCK = 256
 LOG2E = 1.4426950408889634
 HD = 64
 EPS = 1e-06
@@ -189,6 +190,18 @@
     return jnp.exp2(jnp.concatenate(lines, axis=0)).astype(BF16)
 
 
+def merge_both_kernel(near_ref, far_ref, near_x_ref, far_x_ref, out_ref):
+    width = far_ref.shape[1]
+    add_far(near_ref, far_ref, out_ref.at[:, pl.ds(0, width)])
+    add_far(near_x_ref, far_x_ref, out_ref.at[:, pl.ds(width, width)])
+
+
+def merge_both(near, far, near_x, far_x):
+    rows, width = far.shape
+    shape = (jax.ShapeDtypeStruct((rows, 2 * width), BF16),)
+    return local_call(merge_both_kernel, 1000000, shape, near, far, near_x, far_x)[0]
+
+
 def add_far(near_ref, far_ref, out_ref):
     rows, width = far_ref.shape
     heads = width // HD
@@ -340,6 +353,71 @@
     )(*flat)
 
 
+def stacks_of(plan, refs):
+    depth = refs[0].shape[1] // len(plan)
+    at, stacks = 1, []
+    for i, (pieces, flips) in enumerate(plan):
+        stacks.append((refs[0][:, pl.ds(i * depth, depth)], refs[at : at + pieces], flips))
+        at += pieces
+    return stacks
+
+
+def columns_of(stacks, columns, total):
+    for left, pieces, flips in stacks:
+        right = [piece[:, columns] for piece in pieces]
+        for k in range(0, flips, 2):
+            keep = lax.axis_index("grp") == 0
+            one, two = right[k : k + 2]
+            right[k : k + 2] = [jnp.where(keep, one, two), jnp.where(keep, two, one)]
+        total += jnp.dot(left, jnp.concatenate(right, axis=0), preferred_element_type=F32)
+    return total
+
+
+def early_kernel(plan, block, *refs):
+    out_ref = refs[-1]
+    rows, model = out_ref.shape
+    stacks = stacks_of(plan, refs[:-1])
+    for j in range(0, model, block):
+        columns = pl.ds(j, block)
+        out_ref[:, columns] = columns_of(stacks, columns, jnp.zeros((rows, block), F32))
+
+
+def late_kernel(plan, block, early_ref, *refs):
+    out_hbm, staged, sems = refs[-3:]
+    model = staged.shape[1]
+    stacks = stacks_of(plan, refs[:-3])
+    copies = []
+    for j in range(0, model, block):
+        columns = pl.ds(j, block)
+        staged[:, columns] = columns_of(stacks, columns, early_ref[:, columns]).astype(BF16)
+        copies.append(pltpu.make_async_copy(staged.at[:, columns], out_hbm.at[:, columns], sems.at[j // block]))
+        copies[-1].start()
+    for copy in copies:
+        copy.wait()
+
+
+def summed_output(results, groups, early):
+    plan = tuple((len(pieces), flips) for pieces, flips in groups)
+    flat = [results] + [x for pieces, _ in groups for x in pieces]
+    rows = results.shape[0]
+    model = flat[1].shape[1]
+    block = LATE_BLOCK if model % LATE_BLOCK == 0 else model
+    if early is None:
+        kernel, operands, dtype, scratch = early_kernel, flat, F32, []
+    else:
+        kernel, operands, dtype = late_kernel, [early] + flat, BF16
+        scratch = [pltpu.VMEM((rows, model), BF16), pltpu.SemaphoreType.DMA((model // block,))]
+    return pl.pallas_call(
+        functools.partial(kernel, plan, block),
+        out_shape=jax.ShapeDtypeStruct((rows, model), dtype),
+        in_specs=[VMEM_SPEC] * len(operands),
+        out_specs=VMEM_SPEC if early is None else HBM_SPEC,
+        scratch_shapes=scratch,
+        cost_estimate=cost(2 * rows * model * results.shape[1]),
+        compiler_params=params(6),
+    )(*operands)
+
+
 def finish_kernel(span, mine_ref, theirs_ref, out_hbm, staged, sems):
     copies = []
     for i in range(staged.shape[0] // span):
@@ -433,6 +511,9 @@
         first = tie(first, states[0][1])
         second = lax.ppermute(first, "grp", [(0, 1), (1, 0)])
         weights = weights + [[first, second, half]]
+        if split:
+            own_core = swap(tie(w_out, states[0][1]), bits[-1])
+            first_core = swap(tie(first, states[0][1]), bits[-1])
     for i, block in enumerate(arrived):
         last = i == len(arrived) - 1
         if i == 0 and split:
@@ -465,6 +546,14 @@
             far = [None]
     for bit in bits[:-1]:
         near = near + [swap(x, bit) for x in near]
+    if len(far) == 2 and shared:
+        half_core = swap(tie(half, states[0]), bits[-1])
+        second_core = swap(tie(second, states[0]), bits[-1])
+        both = merge_both(near[0], far[0], near[1], far[1])
+        both_core = swap(both, bits[-1])
+        early = summed_output(both, [([w_out], 0), (weights[1], 2)], None)
+        cores = [([own_core], 0), ([first_core, second_core, half_core], 2)]
+        return summed_output(both_core, cores, early)
     if len(far) == 2:
         near[1], far[1] = merge(near[1], far[1]), None
     far = far + [None] * (len(near) - len(far))

time: 31.7 us -> 44.1 us (1.39)
  the two profiles are of different devices: /device:TPU:25 before, /device:TPU:17 now
where the time goes in v2:
time: 44.1 us; the launch traced here: 43.9 us
  waiting for transfers between devices  18.7 us (42%)
  starting transfers between devices  15.7 us (36%)
  Pallas kernels  9.39 us (21%)
    ppermute x8, starting transfers between devices, swap(): return lax.ppermute(x, 'tp', [(i, i ^ bit) for i in range(group)])  10.2 us
    ppermute x8, waiting for transfers between devices, swap(): return lax.ppermute(x, 'tp', [(i, i ^ bit) for i in range(group)])  8.44 us
    ppermute x1, waiting for transfers between devices, layer(): far.append(lax.ppermute(states[1], ('sp', 'tp'), both))  3.93 us
    ppermute x1, waiting for transfers between devices, layer(): last_q = lax.ppermute(q, 'sp', [(shards - 1, shards - 2)])  3.42 us
    pallas_call x6, Pallas kernels, local_call(): pl.pallas_call(kernel, out_shape=out_shape, in_specs=[VMEM_SPEC] * len(op...  2.9 us
    pallas_call x2, Pallas kernels, summed_output(): pl.pallas_call(functools.partial(kernel, plan, block), out_shape=jax.Shap...  2.88 us
    ppermute x1, waiting for transfers between devices, layer(): far = [lax.ppermute(states[1], 'sp', pairs)]  2.8 us
    pallas_call x1, Pallas kernels, project(): pl.pallas_call(functools.partial(project_kernel, chunks), out_shape=(pack...  2.64 us
  transfers between devices with their start and end apart: 14, of which 6 were waited for; matrix products, arithmetic and copies ran while one was open for 0% of the time, Pallas kernels for 11%

profile of v2, /device:TPU:17, one launch (start us, length us, event | category | flops | bytes accessed | tf_op | source)
XLA Modules:
  0.0 43.9 jit_solution(2238761283651367888)
XLA Ops:
  0.0 2.6 %project.1 = (bf16[136,512]{1,0:T(8,128)(2,1)S(1)}, bf16[128,256]{1,0:T(8,128)(2,1)S(1)}, bf16[96,2048]{1,0:T(8,128)(2,1)S(1)}) custom-call(bf16[128,2048]{1,0:T(8,128)(2,1)} %tok_hbm.1, f32[1,2048]{1,0:T(1,128)} %bitcast.1, bf16[4,128]{1,0:T(4,128)(2,1)} %rate_hbm.1, bf16[2048,256]{1,0:T(8,128)(2,1)} %wk_hbm.1, bf16[2048,256]{1,0:T(8,128)(2,1)} %wv_hbm.1, ...), custom_call_target="tpu_custom_call" | custom-call | flops 402653184 | bytes 1048576 | tf_op jit(solution)/shard_map/project/pallas_call | solution.py:84
  2.6 0.6 %shard_map.73 = (f32[128,256]{1,0:T(8,128)S(1)}, f32[512,128]{1,0:T(8,128)S(1)}) custom-call(bf16[128,256]{1,0:T(8,128)(2,1)S(1)} %get-tuple-element.21.q_ref.refs_0_, bf16[136,512]{1,0:T(8,128)(2,1)S(1)} %get-tuple-element.20.kv_ref), custom_call_target="tpu_custom_call" | custom-call | flops 600000000 | bytes 1048576 | tf_op jit(solution)/shard_map/pallas_call | solution.py:271
  3.2 0.7 %collective-permute-start.10 = (bf16[256,2048]{1,0:T(8,128)(2,1)}, bf16[256,2048]{1,0:T(8,128)(2,1)S(1)}, u32[]{:S(2)}, u32[]{:S(2)}) collective-permute-start(bf16[256,2048]{1,0:T(8,128)(2,1)} %refs_1_.1), channel_id=1, source_target_pairs={{0,1},{1,0},{2,3},{3,2},{4,5},{5,4},{6,7},{7,6},{8,9},{9,8},{10,11... | collective-permute-start | bytes 3145736 | tf_op jit(solution)/shard_map/ppermute | solution.py:482
  4.0 1.0 %cut.1 = bf16[80,2048]{1,0:T(8,128)(2,1)S(1)} custom-call(bf16[256,2048]{1,0:T(8,128)(2,1)} %refs_1_.1), custom_call_target="tpu_custom_call" | custom-call | flops 1000000 | bytes 1048576 | tf_op jit(solution)/shard_map/cut/pallas_call | solution.py:456
  5.0 1.3 %collective-permute-start.6 = (bf16[80,2048]{1,0:T(8,128)(2,1)S(1)}, bf16[80,2048]{1,0:T(8,128)(2,1)S(1)}, u32[]{:S(2)}, u32[]{:S(2)}) collective-permute-start(bf16[80,2048]{1,0:T(8,128)(2,1)S(1)} %cut.1), channel_id=1, source_target_pairs={{0,2},{1,3},{2,0},{3,1},{4,6},{5,7},{6,4},{7,5},{8,10},{9,11},{10,... | collective-permute-start | bytes 983048 | tf_op jit(solution)/shard_map/ppermute | solution.py:482
  6.2 0.3 collective-permute-start.8
  6.5 1.3 %collective-permute-start.1 = (bf16[136,512]{1,0:T(8,128)(2,1)S(1)}, bf16[136,512]{1,0:T(8,128)(2,1)S(1)}, u32[]{:S(2)}, u32[]{:S(2)}) collective-permute-start(bf16[136,512]{1,0:T(8,128)(2,1)S(1)} %get-tuple-element.20.kv_ref), channel_id=1, source_target_pairs={{0,4},{4,8},{8,12},{12,0},{1,5},{5,9},{9,13},{13,1},{2,6},{6,10},{... | collective-permute-start | bytes 417800 | tf_op jit(solution)/shard_map/ppermute | solution.py:506
  7.8 6.5 %collective-permute-done.6.refs_2_ = bf16[80,2048]{1,0:T(8,128)(2,1)S(1)} collective-permute-done((bf16[80,2048]{1,0:T(8,128)(2,1)S(1)}, bf16[80,2048]{1,0:T(8,128)(2,1)S(1)}, u32[]{:S(2)}, u32[]{:S(2)}) %collective-permute-start.6) | collective-permute-done | bytes 327712 | tf_op jit(solution)/shard_map/ppermute | solution.py:482
  14.3 1.2 %collective-permute-start.7 = (bf16[80,2048]{1,0:T(8,128)(2,1)S(1)}, bf16[80,2048]{1,0:T(8,128)(2,1)S(1)}, u32[]{:S(2)}, u32[]{:S(2)}) collective-permute-start(bf16[80,2048]{1,0:T(8,128)(2,1)S(1)} %collective-permute-done.6.refs_2_), channel_id=1, source_target_pairs={{0,16},{16,0},{1,17},{17,1},{2,18},{18,2},{3,19},{19,3},{4,20},{20... | collective-permute-start | bytes 983048 | tf_op jit(solution)/shard_map/ppermute | solution.py:512
  15.5 1.3 %collective-permute-start = (bf16[136,512]{1,0:T(8,128)(2,1)S(1)}, bf16[136,512]{1,0:T(8,128)(2,1)S(1)}, u32[]{:S(2)}, u32[]{:S(2)}) collective-permute-start(bf16[136,512]{1,0:T(8,128)(2,1)S(1)} %get-tuple-element.20.kv_ref), channel_id=1, source_target_pairs={{0,8},{1,9},{2,10},{3,11},{16,24},{17,25},{18,26},{19,27}} | collective-permute-start | bytes 417800 | tf_op jit(solution)/shard_map/ppermute | solution.py:506
  16.8 0.0 collective-permute-done.1.kv_ref
  16.8 1.3 %collective-permute-start.2 = (bf16[128,256]{1,0:T(8,128)(2,1)S(1)}, bf16[128,256]{1,0:T(8,128)(2,1)S(1)}, u32[]{:S(2)}, u32[]{:S(2)}) collective-permute-start(bf16[128,256]{1,0:T(8,128)(2,1)S(1)} %get-tuple-element.21.q_ref.refs_0_), channel_id=1, source_target_pairs={{12,8},{13,9},{14,10},{15,11},{28,24},{29,25},{30,26},{31,27}} | collective-permute-start | bytes 196616 | tf_op jit(solution)/shard_map/ppermute | solution.py:508
  18.1 0.6 %shard_map.74 = (f32[128,256]{1,0:T(8,128)S(1)}, f32[512,128]{1,0:T(8,128)S(1)}) custom-call(bf16[136,512]{1,0:T(8,128)(2,1)S(1)} %collective-permute-done.1.kv_ref, bf16[128,256]{1,0:T(8,128)(2,1)S(1)} %get-tuple-element.21.q_ref.refs_0_, f32[128,256]{1,0:T(8,128)S(1)} %get-tuple-element.22.refs_1_, f32[512,128]{1,0:T(8,128)S(1)} %get-tuple-element.23.refs_2_), custom_call_target="tpu_custom_call" | custom-call | flops 600000000 | bytes 1048576 | tf_op jit(solution)/shard_map/pallas_call | solution.py:271
  18.7 3.4 %collective-permute-done.2.q_ref.refs_0_ = bf16[128,256]{1,0:T(8,128)(2,1)S(1)} collective-permute-done((bf16[128,256]{1,0:T(8,128)(2,1)S(1)}, bf16[128,256]{1,0:T(8,128)(2,1)S(1)}, u32[]{:S(2)}, u32[]{:S(2)}) %collective-permute-start.2) | collective-permute-done | bytes 65568 | tf_op jit(solution)/shard_map/ppermute | solution.py:508
  22.1 0.1 collective-permute-done.kv_ref
  22.2 0.6 %shard_map.75.near_ref = bf16[136,256]{1,0:T(8,128)(2,1)S(1)} custom-call(bf16[136,512]{1,0:T(8,128)(2,1)S(1)} %collective-permute-done.kv_ref, bf16[128,256]{1,0:T(8,128)(2,1)S(1)} %get-tuple-element.21.q_ref.refs_0_, f32[128,256]{1,0:T(8,128)S(1)} %get-tuple-element.24.refs_1_, f32[512,128]{1,0:T(8,128)S(1)} %get-tuple-element.25.refs_2_), custom_call_target="tpu_custom_call" | custom-call | flops 600000000 | bytes 1048576 | tf_op jit(solution)/shard_map/pallas_call | solution.py:271
  22.8 0.0 collective-permute-done.8.refs_4_
  22.8 2.9 %collective-permute-start.13 = (bf16[96,2048]{1,0:T(8,128)(2,1)S(1)}, bf16[96,2048]{1,0:T(8,128)(2,1)S(1)}, u32[]{:S(2)}, u32[]{:S(2)}) collective-permute-start(bf16[96,2048]{1,0:T(8,128)(2,1)S(1)} %collective-permute-done.8.refs_4_), channel_id=1, source_target_pairs={{0,1},{1,0},{2,3},{3,2},{4,5},{5,4},{6,7},{7,6},{8,9},{9,8},{10,11... | collective-permute-start | bytes 1179656 | tf_op jit(solution)/shard_map/ppermute | solution.py:482
  25.7 0.6 %shard_map.76 = (f32[128,256]{1,0:T(8,128)S(1)}, f32[512,128]{1,0:T(8,128)S(1)}) custom-call(bf16[128,256]{1,0:T(8,128)(2,1)S(1)} %collective-permute-done.2.q_ref.refs_0_, bf16[136,512]{1,0:T(8,128)(2,1)S(1)} %collective-permute-done.1.kv_ref), custom_call_target="tpu_custom_call" | custom-call | flops 600000000 | bytes 1048576 | tf_op jit(solution)/shard_map/pallas_call | solution.py:271
  26.2 0.6 %shard_map.77 = bf16[128,256]{1,0:T(8,128)(2,1)S(1)} custom-call(bf16[136,512]{1,0:T(8,128)(2,1)S(1)} %collective-permute-done.kv_ref, bf16[128,256]{1,0:T(8,128)(2,1)S(1)} %collective-permute-done.2.q_ref.refs_0_, f32[128,256]{1,0:T(8,128)S(1)} %get-tuple-element.27.refs_1_, f32[512,128]{1,0:T(8,128)S(1)} %get-tuple-element.28.refs_2_), custom_call_target="tpu_custom_call" | custom-call | flops 600000000 | bytes 1048576 | tf_op jit(solution)/shard_map/pallas_call | solution.py:271
  26.8 0.1 collective-permute-start.5
  26.9 0.1 collective-permute-start.11
  27.0 0.0 collective-permute-done.7.refs_3_
  27.0 0.5 %collective-permute-start.12 = (bf16[80,2048]{1,0:T(8,128)(2,1)S(1)}, bf16[80,2048]{1,0:T(8,128)(2,1)S(1)}, u32[]{:S(2)}, u32[]{:S(2)}) collective-permute-start(bf16[80,2048]{1,0:T(8,128)(2,1)S(1)} %collective-permute-done.7.refs_3_), channel_id=1, source_target_pairs={{0,1},{1,0},{2,3},{3,2},{4,5},{5,4},{6,7},{7,6},{8,9},{9,8},{10,11... | collective-permute-start | bytes 983048 | tf_op jit(solution)/shard_map/ppermute | solution.py:482
  27.5 3.9 %collective-permute-done.5.far_x_ref = bf16[128,256]{1,0:T(8,128)(2,1)S(1)} collective-permute-done((bf16[128,256]{1,0:T(8,128)(2,1)S(1)}, bf16[128,256]{1,0:T(8,128)(2,1)S(1)}, u32[]{:S(2)}, u32[]{:S(2)}) %collective-permute-start.5) | collective-permute-done | bytes 65568 | tf_op jit(solution)/shard_map/ppermute | solution.py:543
  31.4 0.3 collective-permute-start.3
  31.7 2.8 %collective-permute-done.3.far_ref = bf16[128,256]{1,0:T(8,128)(2,1)S(1)} collective-permute-done((bf16[128,256]{1,0:T(8,128)(2,1)S(1)}, bf16[128,256]{1,0:T(8,128)(2,1)S(1)}, u32[]{:S(2)}, u32[]{:S(2)}) %collective-permute-start.3) | collective-permute-done | bytes 65568 | tf_op jit(solution)/shard_map/ppermute | solution.py:540
  34.5 1.2 %collective-permute-start.4 = (bf16[136,256]{1,0:T(8,128)(2,1)S(1)}, bf16[136,256]{1,0:T(8,128)(2,1)S(1)}, u32[]{:S(2)}, u32[]{:S(2)}) collective-permute-start(bf16[136,256]{1,0:T(8,128)(2,1)S(1)} %shard_map.75.near_ref), channel_id=1, source_target_pairs={{0,2},{1,3},{2,0},{3,1},{4,6},{5,7},{6,4},{7,5},{8,10},{9,11},{10,... | collective-permute-start | bytes 208904 | tf_op jit(solution)/shard_map/ppermute | solution.py:482
  35.7 2.0 %collective-permute-done.4.near_x_ref = bf16[136,256]{1,0:T(8,128)(2,1)S(1)} collective-permute-done((bf16[136,256]{1,0:T(8,128)(2,1)S(1)}, bf16[136,256]{1,0:T(8,128)(2,1)S(1)}, u32[]{:S(2)}, u32[]{:S(2)}) %collective-permute-start.4) | collective-permute-done | bytes 69664 | tf_op jit(solution)/shard_map/ppermute | solution.py:482
  37.7 3.2 %collective-permute-start.9 = (bf16[128,512]{1,0:T(8,128)(2,1)S(1)}, bf16[128,512]{1,0:T(8,128)(2,1)S(1)}, u32[]{:S(2)}, u32[]{:S(2)}) collective-permute-start(bf16[128,512]{1,0:T(8,128)(2,1)S(1)} %shard_map.78.refs_0_), channel_id=1, source_target_pairs={{0,1},{1,0},{2,3},{3,2},{4,5},{5,4},{6,7},{7,6},{8,9},{9,8},{10,11... | collective-permute-start | bytes 393224 | tf_op jit(solution)/shard_map/ppermute | solution.py:482
  41.0 1.7 %shard_map.79.early_ref = f32[128,2048]{1,0:T(8,128)S(1)} custom-call(bf16[128,512]{1,0:T(8,128)(2,1)S(1)} %shard_map.78.refs_0_, bf16[256,2048]{1,0:T(8,128)(2,1)} %refs_1_.1, bf16[80,2048]{1,0:T(8,128)(2,1)S(1)} %collective-permute-done.6.refs_2_, bf16[80,2048]{1,0:T(8,128)(2,1)S(1)} %collective-permute-done.7.refs_3_, ...), custom_call_target="tpu_custom_call" | custom-call | flops 268435456 | bytes 1048576 | tf_op jit(solution)/shard_map/pallas_call | solution.py:410
  42.6 0.0 collective-permute-done.9.refs_0_
  42.7 0.0 collective-permute-done.11.refs_2_
  42.7 0.0 collective-permute-done.13.refs_4_
  42.7 0.0 collective-permute-done.12.refs_3_
  42.7 0.0 collective-permute-done.10.refs_1_
  42.7 1.2 %shard_map.80 = bf16[128,2048]{1,0:T(8,128)(2,1)} custom-call(f32[128,2048]{1,0:T(8,128)S(1)} %shard_map.79.early_ref, bf16[128,512]{1,0:T(8,128)(2,1)S(1)} %collective-permute-done.9.refs_0_, bf16[256,2048]{1,0:T(8,128)(2,1)S(1)} %collective-permute-done.10.refs_1_, bf16[80,2048]{1,0:T(8,128)(2,1)S(1)} %collective-permute-done.11.refs_2_, ...), custom_call_target="tpu_custom_call" | custom-call | flops 268435456 | bytes 1048576 | tf_op jit(solution)/shard_map/pallas_call | solution.py:410
  (1 shorter events, 0.0 us)
Async XLA Ops:
  3.2 39.4 %collective-permute-start.10 = (bf16[256,2048]{1,0:T(8,128)(2,1)}, bf16[256,2048]{1,0:T(8,128)(2,1)S(1)}, u32[]{:S(2)}, u32[]{:S(2)}) collective-permute-start(bf16[256,2048]{1,0:T(8,128)(2,1)} %refs_1_.1), channel_id=1, source_target_pairs={{0,1},{1,0},{2,3},{3,2},{4,5},{5,4},{6,7},{7,6},{8,9},{9,8},{10,11... | collective-permute-start | bytes 3145736 | tf_op jit(solution)/shard_map/ppermute | solution.py:482
  5.0 9.3 %collective-permute-start.6 = (bf16[80,2048]{1,0:T(8,128)(2,1)S(1)}, bf16[80,2048]{1,0:T(8,128)(2,1)S(1)}, u32[]{:S(2)}, u32[]{:S(2)}) collective-permute-start(bf16[80,2048]{1,0:T(8,128)(2,1)S(1)} %cut.1), channel_id=1, source_target_pairs={{0,2},{1,3},{2,0},{3,1},{4,6},{5,7},{6,4},{7,5},{8,10},{9,11},{10,... | collective-permute-start | bytes 983048 | tf_op jit(solution)/shard_map/ppermute | solution.py:482
  6.2 16.5 %collective-permute-start.8 = (bf16[96,2048]{1,0:T(8,128)(2,1)S(1)}, bf16[96,2048]{1,0:T(8,128)(2,1)S(1)}, u32[]{:S(2)}, u32[]{:S(2)}) collective-permute-start(bf16[96,2048]{1,0:T(8,128)(2,1)S(1)} %get-tuple-element.30), channel_id=1, source_target_pairs={{0,2},{1,3},{2,0},{3,1},{4,6},{5,7},{6,4},{7,5},{8,10},{9,11},{10,... | collective-permute-start | bytes 1179656 | tf_op jit(solution)/shard_map/ppermute | solution.py:482
  6.5 10.3 %collective-permute-start.1 = (bf16[136,512]{1,0:T(8,128)(2,1)S(1)}, bf16[136,512]{1,0:T(8,128)(2,1)S(1)}, u32[]{:S(2)}, u32[]{:S(2)}) collective-permute-start(bf16[136,512]{1,0:T(8,128)(2,1)S(1)} %get-tuple-element.20.kv_ref), channel_id=1, source_target_pairs={{0,4},{4,8},{8,12},{12,0},{1,5},{5,9},{9,13},{13,1},{2,6},{6,10},{... | collective-permute-start | bytes 417800 | tf_op jit(solution)/shard_map/ppermute | solution.py:506
  14.3 12.7 %collective-permute-start.7 = (bf16[80,2048]{1,0:T(8,128)(2,1)S(1)}, bf16[80,2048]{1,0:T(8,128)(2,1)S(1)}, u32[]{:S(2)}, u32[]{:S(2)}) collective-permute-start(bf16[80,2048]{1,0:T(8,128)(2,1)S(1)} %collective-permute-done.6.refs_2_), channel_id=1, source_target_pairs={{0,16},{16,0},{1,17},{17,1},{2,18},{18,2},{3,19},{19,3},{4,20},{20... | collective-permute-start | bytes 983048 | tf_op jit(solution)/shard_map/ppermute | solution.py:512
  15.5 6.7 %collective-permute-start = (bf16[136,512]{1,0:T(8,128)(2,1)S(1)}, bf16[136,512]{1,0:T(8,128)(2,1)S(1)}, u32[]{:S(2)}, u32[]{:S(2)}) collective-permute-start(bf16[136,512]{1,0:T(8,128)(2,1)S(1)} %get-tuple-element.20.kv_ref), channel_id=1, source_target_pairs={{0,8},{1,9},{2,10},{3,11},{16,24},{17,25},{18,26},{19,27}} | collective-permute-start | bytes 417800 | tf_op jit(solution)/shard_map/ppermute | solution.py:506
  16.8 5.3 %collective-permute-start.2 = (bf16[128,256]{1,0:T(8,128)(2,1)S(1)}, bf16[128,256]{1,0:T(8,128)(2,1)S(1)}, u32[]{:S(2)}, u32[]{:S(2)}) collective-permute-start(bf16[128,256]{1,0:T(8,128)(2,1)S(1)} %get-tuple-element.21.q_ref.refs_0_), channel_id=1, source_target_pairs={{12,8},{13,9},{14,10},{15,11},{28,24},{29,25},{30,26},{31,27}} | collective-permute-start | bytes 196616 | tf_op jit(solution)/shard_map/ppermute | solution.py:508
  22.8 19.9 %collective-permute-start.13 = (bf16[96,2048]{1,0:T(8,128)(2,1)S(1)}, bf16[96,2048]{1,0:T(8,128)(2,1)S(1)}, u32[]{:S(2)}, u32[]{:S(2)}) collective-permute-start(bf16[96,2048]{1,0:T(8,128)(2,1)S(1)} %collective-permute-done.8.refs_4_), channel_id=1, source_target_pairs={{0,1},{1,0},{2,3},{3,2},{4,5},{5,4},{6,7},{7,6},{8,9},{9,8},{10,11... | collective-permute-start | bytes 1179656 | tf_op jit(solution)/shard_map/ppermute | solution.py:482
  26.8 4.6 %collective-permute-start.5 = (bf16[128,256]{1,0:T(8,128)(2,1)S(1)}, bf16[128,256]{1,0:T(8,128)(2,1)S(1)}, u32[]{:S(2)}, u32[]{:S(2)}) collective-permute-start(bf16[128,256]{1,0:T(8,128)(2,1)S(1)} %shard_map.77), channel_id=1, source_target_pairs={{0,6},{1,7},{2,4},{3,5},{4,2},{5,3},{6,0},{7,1},{8,14},{9,15},{10,... | collective-permute-start | bytes 196616 | tf_op jit(solution)/shard_map/ppermute | solution.py:543
  26.9 15.8 %collective-permute-start.11 = (bf16[80,2048]{1,0:T(8,128)(2,1)S(1)}, bf16[80,2048]{1,0:T(8,128)(2,1)S(1)}, u32[]{:S(2)}, u32[]{:S(2)}) collective-permute-start(bf16[80,2048]{1,0:T(8,128)(2,1)S(1)} %collective-permute-done.6.refs_2_), channel_id=1, source_target_pairs={{0,1},{1,0},{2,3},{3,2},{4,5},{5,4},{6,7},{7,6},{8,9},{9,8},{10,11... | collective-permute-start | bytes 983048 | tf_op jit(solution)/shard_map/ppermute | solution.py:482
  27.0 15.7 %collective-permute-start.12 = (bf16[80,2048]{1,0:T(8,128)(2,1)S(1)}, bf16[80,2048]{1,0:T(8,128)(2,1)S(1)}, u32[]{:S(2)}, u32[]{:S(2)}) collective-permute-start(bf16[80,2048]{1,0:T(8,128)(2,1)S(1)} %collective-permute-done.7.refs_3_), channel_id=1, source_target_pairs={{0,1},{1,0},{2,3},{3,2},{4,5},{5,4},{6,7},{7,6},{8,9},{9,8},{10,11... | collective-permute-start | bytes 983048 | tf_op jit(solution)/shard_map/ppermute | solution.py:482
  31.4 3.1 %collective-permute-start.3 = (bf16[128,256]{1,0:T(8,128)(2,1)S(1)}, bf16[128,256]{1,0:T(8,128)(2,1)S(1)}, u32[]{:S(2)}, u32[]{:S(2)}) collective-permute-start(bf16[128,256]{1,0:T(8,128)(2,1)S(1)} %shard_map.77), channel_id=1, source_target_pairs={{0,4},{4,0},{8,12},{12,8},{1,5},{5,1},{9,13},{13,9},{2,6},{6,2},{1... | collective-permute-start | bytes 196616 | tf_op jit(solution)/shard_map/ppermute | solution.py:540
  34.5 3.2 %collective-permute-start.4 = (bf16[136,256]{1,0:T(8,128)(2,1)S(1)}, bf16[136,256]{1,0:T(8,128)(2,1)S(1)}, u32[]{:S(2)}, u32[]{:S(2)}) collective-permute-start(bf16[136,256]{1,0:T(8,128)(2,1)S(1)} %shard_map.75.near_ref), channel_id=1, source_target_pairs={{0,2},{1,3},{2,0},{3,1},{4,6},{5,7},{6,4},{7,5},{8,10},{9,11},{10,... | collective-permute-start | bytes 208904 | tf_op jit(solution)/shard_map/ppermute | solution.py:482
  37.7 4.9 %collective-permute-start.9 = (bf16[128,512]{1,0:T(8,128)(2,1)S(1)}, bf16[128,512]{1,0:T(8,128)(2,1)S(1)}, u32[]{:S(2)}, u32[]{:S(2)}) collective-permute-start(bf16[128,512]{1,0:T(8,128)(2,1)S(1)} %shard_map.78.refs_0_), channel_id=1, source_target_pairs={{0,1},{1,0},{2,3},{3,2},{4,5},{5,4},{6,7},{7,6},{8,9},{9,8},{10,11... | collective-permute-start | bytes 393224 | tf_op jit(solution)/shard_map/ppermute | solution.py:482

commit v3 on v2

--- a/solution.py
+++ b/solution.py
@@ -8,7 +8,7 @@
 from jax.sharding import PartitionSpec as P
 
 
-LATE_BLOCK = 256
+LATE_BLOCK = 512
 LOG2E = 1.4426950408889634
 HD = 64
 EPS = 1e-06
@@ -363,23 +363,27 @@
 
 
 def columns_of(stacks, columns, total):
+    lefts, rights = [], []
     for left, pieces, flips in stacks:
         right = [piece[:, columns] for piece in pieces]
         for k in range(0, flips, 2):
             keep = lax.axis_index("grp") == 0
             one, two = right[k : k + 2]
             right[k : k + 2] = [jnp.where(keep, one, two), jnp.where(keep, two, one)]
-        total += jnp.dot(left, jnp.concatenate(right, axis=0), preferred_element_type=F32)
-    return total
+        lefts.append(left)
+        rights += right
+    left, right = jnp.concatenate(lefts, axis=1), jnp.concatenate(rights, axis=0)
+    product = jnp.dot(left, right, preferred_element_type=F32)
+    return product if total is None else product + total
 
 
 def early_kernel(plan, block, *refs):
     out_ref = refs[-1]
-    rows, model = out_ref.shape
+    _, model = out_ref.shape
     stacks = stacks_of(plan, refs[:-1])
     for j in range(0, model, block):
         columns = pl.ds(j, block)
-        out_ref[:, columns] = columns_of(stacks, columns, jnp.zeros((rows, block), F32))
+        out_ref[:, columns] = columns_of(stacks, columns, None)
 
 
 def late_kernel(plan, block, early_ref, *refs):
@@ -444,27 +448,6 @@
     )(mine, theirs)
 
 
-def cut_kernel(w_hbm, first_ref, sem):
-    first = first_ref.shape[0]
-    at = pl.multiple_of(lax.axis_index("grp") * first, first)
-    copy = pltpu.make_async_copy(w_hbm.at[pl.ds(at, first)], first_ref, sem)
-    copy.start()
-    copy.wait()
-
-
-def cut(w_out, share):
-    return pl.pallas_call(
-        cut_kernel,
-        out_shape=pltpu.VMEM((share, w_out.shape[1]), BF16),
-        in_specs=[HBM_SPEC],
-        out_specs=VMEM_SPEC,
-        scratch_shapes=[pltpu.SemaphoreType.DMA],
-        cost_estimate=cost(1000000),
-        compiler_params=params(4),
-        name="cut",
-    )(in_hbm(w_out))
-
-
 def tie(x, after):
     return lax.optimization_barrier((x, after))[0]
 
@@ -486,7 +469,7 @@
     weights = [[w_out]]
     if shared:
         share = depth * 5 // 16
-        first = cut(w_out, share)
+        first = lax.dynamic_slice_in_dim(w_out, lax.axis_index("grp") * share, share, 0)
         first = swap(first, bits[0])
     else:
         for bit in bits[:-1]:

time: 44.1 us -> 42.9 us (0.973)
  Pallas kernels: 9.39 us -> 7.14 us
  local copies, waits for them, and re-layouts: 0 us -> 0.65 us
  waiting for transfers between devices: 18.7 us -> 19.2 us
    pallas_call x2, Pallas kernels: 2.88 us -> 1.61 us  [summed_output(): pl.pallas_call(functools.partial(kernel, plan, block), out_shape=jax.Shap...]
    pallas_call x1 -> x0, Pallas kernels: 0.98 us -> none  [cut(): pl.pallas_call(cut_kernel, out_shape=pltpu.VMEM((share, w_out.shape[1]),...]
    unnamed x0 -> x2, local copies, waits for them, and re-layouts: none -> 0.63 us
    ppermute x8, waiting for transfers between devices: 8.44 us -> 8.98 us  [swap(): return lax.ppermute(x, 'tp', [(i, i ^ bit) for i in range(group)])]
  transfers between devices with their start and end apart: 14 -> 14, of which waited for: 6 -> 7; matrix products, arithmetic and copies ran while one was open for 0% -> 0% of each run, Pallas kernels for 11% -> 6%
where the time goes in v3:
time: 42.9 us; the launch traced here: 42.7 us
  waiting for transfers between devices  19.2 us (45%)
  starting transfers between devices  15.5 us (36%)
  Pallas kernels  7.14 us (17%)
  local copies, waits for them, and re-layouts  0.65 us (2%)
    ppermute x8, starting transfers between devices, swap(): return lax.ppermute(x, 'tp', [(i, i ^ bit) for i in range(group)])  10.1 us
    ppermute x8, waiting for transfers between devices, swap(): return lax.ppermute(x, 'tp', [(i, i ^ bit) for i in range(group)])  8.98 us
    ppermute x1, waiting for transfers between devices, layer(): far.append(lax.ppermute(states[1], ('sp', 'tp'), both))  3.93 us
    ppermute x1, waiting for transfers between devices, layer(): last_q = lax.ppermute(q, 'sp', [(shards - 1, shards - 2)])  3.42 us
    pallas_call x6, Pallas kernels, local_call(): pl.pallas_call(kernel, out_shape=out_shape, in_specs=[VMEM_SPEC] * len(op...  2.89 us
    ppermute x1, waiting for transfers between devices, layer(): far = [lax.ppermute(states[1], 'sp', pairs)]  2.8 us
    pallas_call x1, Pallas kernels, project(): pl.pallas_call(functools.partial(project_kernel, chunks), out_shape=(pack...  2.64 us
    ppermute x2, starting transfers between devices, layer(): arrived.append(lax.ppermute(kv, 'sp', pairs))  2.58 us
  transfers between devices with their start and end apart: 14, of which 7 were waited for; matrix products, arithmetic and copies ran while one was open for 0% of the time, Pallas kernels for 6%

profile of v3, /device:TPU:17, one launch (start us, length us, event | category | flops | bytes accessed | tf_op | source)
XLA Modules:
  0.0 42.7 jit_solution(15825974483990113466)
XLA Ops:
  0.0 2.6 %project.1 = (bf16[136,512]{1,0:T(8,128)(2,1)S(1)}, bf16[128,256]{1,0:T(8,128)(2,1)S(1)}, bf16[96,2048]{1,0:T(8,128)(2,1)S(1)}) custom-call(bf16[128,2048]{1,0:T(8,128)(2,1)} %tok_hbm.1, f32[1,2048]{1,0:T(1,128)} %bitcast.1, bf16[4,128]{1,0:T(4,128)(2,1)} %rate_hbm.1, bf16[2048,256]{1,0:T(8,128)(2,1)} %wk_hbm.1, bf16[2048,256]{1,0:T(8,128)(2,1)} %wv_hbm.1, ...), custom_call_target="tpu_custom_call" | custom-call | flops 402653184 | bytes 1048576 | tf_op jit(solution)/shard_map/project/pallas_call | solution.py:84
  2.6 0.0 copy-start
  2.7 0.6 %shard_map.73 = (f32[128,256]{1,0:T(8,128)S(1)}, f32[512,128]{1,0:T(8,128)S(1)}) custom-call(bf16[128,256]{1,0:T(8,128)(2,1)S(1)} %get-tuple-element.21.q_ref.refs_0_, bf16[136,512]{1,0:T(8,128)(2,1)S(1)} %get-tuple-element.20.kv_ref), custom_call_target="tpu_custom_call" | custom-call | flops 600000000 | bytes 1048576 | tf_op jit(solution)/shard_map/pallas_call | solution.py:271
  3.3 0.6 %copy-done = bf16[256,2048]{1,0:T(8,128)(2,1)S(1)} copy-done((bf16[256,2048]{1,0:T(8,128)(2,1)S(1)}, bf16[256,2048]{1,0:T(8,128)(2,1)}, u32[]{:S(2)}) %copy-start) | copy-done | bytes 1048600
  3.9 0.7 %collective-permute-start.10 = (bf16[256,2048]{1,0:T(8,128)(2,1)S(1)}, bf16[256,2048]{1,0:T(8,128)(2,1)S(1)}, u32[]{:S(2)}, u32[]{:S(2)}) collective-permute-start(bf16[256,2048]{1,0:T(8,128)(2,1)S(1)} %copy-done), channel_id=1, source_target_pairs={{0,1},{1,0},{2,3},{3,2},{4,5},{5,4},{6,7},{7,6},{8,9},{9,8},{10,11... | collective-permute-start | bytes 3145736 | tf_op jit(solution)/shard_map/ppermute | solution.py:465
  4.6 1.3 %collective-permute-start.6 = (bf16[80,2048]{1,0:T(8,128)(2,1)S(1)}, bf16[80,2048]{1,0:T(8,128)(2,1)S(1)}, u32[]{:S(2)}, u32[]{:S(2)}) collective-permute-start(bf16[80,2048]{1,0:T(8,128)(2,1)S(1)} %constant_dynamic-slice_fusion), channel_id=1, source_target_pairs={{0,2},{1,3},{2,0},{3,1},{4,6},{5,7},{6,4},{7,5},{8,10},{9,11},{10,... | collective-permute-start | bytes 983048 | tf_op jit(solution)/shard_map/ppermute | solution.py:465
  5.9 0.3 collective-permute-start.8
  6.1 1.3 %collective-permute-start.1 = (bf16[136,512]{1,0:T(8,128)(2,1)S(1)}, bf16[136,512]{1,0:T(8,128)(2,1)S(1)}, u32[]{:S(2)}, u32[]{:S(2)}) collective-permute-start(bf16[136,512]{1,0:T(8,128)(2,1)S(1)} %get-tuple-element.20.kv_ref), channel_id=1, source_target_pairs={{0,4},{4,8},{8,12},{12,0},{1,5},{5,9},{9,13},{13,1},{2,6},{6,10},{... | collective-permute-start | bytes 417800 | tf_op jit(solution)/shard_map/ppermute | solution.py:489
  7.4 6.5 %collective-permute-done.6.refs_2_ = bf16[80,2048]{1,0:T(8,128)(2,1)S(1)} collective-permute-done((bf16[80,2048]{1,0:T(8,128)(2,1)S(1)}, bf16[80,2048]{1,0:T(8,128)(2,1)S(1)}, u32[]{:S(2)}, u32[]{:S(2)}) %collective-permute-start.6) | collective-permute-done | bytes 327712 | tf_op jit(solution)/shard_map/ppermute | solution.py:465
  13.9 1.2 %collective-permute-start.7 = (bf16[80,2048]{1,0:T(8,128)(2,1)S(1)}, bf16[80,2048]{1,0:T(8,128)(2,1)S(1)}, u32[]{:S(2)}, u32[]{:S(2)}) collective-permute-start(bf16[80,2048]{1,0:T(8,128)(2,1)S(1)} %collective-permute-done.6.refs_2_), channel_id=1, source_target_pairs={{0,16},{16,0},{1,17},{17,1},{2,18},{18,2},{3,19},{19,3},{4,20},{20... | collective-permute-start | bytes 983048 | tf_op jit(solution)/shard_map/ppermute | solution.py:495
  15.1 1.3 %collective-permute-start = (bf16[136,512]{1,0:T(8,128)(2,1)S(1)}, bf16[136,512]{1,0:T(8,128)(2,1)S(1)}, u32[]{:S(2)}, u32[]{:S(2)}) collective-permute-start(bf16[136,512]{1,0:T(8,128)(2,1)S(1)} %get-tuple-element.20.kv_ref), channel_id=1, source_target_pairs={{0,8},{1,9},{2,10},{3,11},{16,24},{17,25},{18,26},{19,27}} | collective-permute-start | bytes 417800 | tf_op jit(solution)/shard_map/ppermute | solution.py:489
  16.4 0.0 collective-permute-done.1.kv_ref
  16.4 1.3 %collective-permute-start.2 = (bf16[128,256]{1,0:T(8,128)(2,1)S(1)}, bf16[128,256]{1,0:T(8,128)(2,1)S(1)}, u32[]{:S(2)}, u32[]{:S(2)}) collective-permute-start(bf16[128,256]{1,0:T(8,128)(2,1)S(1)} %get-tuple-element.21.q_ref.refs_0_), channel_id=1, source_target_pairs={{12,8},{13,9},{14,10},{15,11},{28,24},{29,25},{30,26},{31,27}} | collective-permute-start | bytes 196616 | tf_op jit(solution)/shard_map/ppermute | solution.py:491
  17.7 0.6 %shard_map.74 = (f32[128,256]{1,0:T(8,128)S(1)}, f32[512,128]{1,0:T(8,128)S(1)}) custom-call(bf16[136,512]{1,0:T(8,128)(2,1)S(1)} %collective-permute-done.1.kv_ref, bf16[128,256]{1,0:T(8,128)(2,1)S(1)} %get-tuple-element.21.q_ref.refs_0_, f32[128,256]{1,0:T(8,128)S(1)} %get-tuple-element.22.refs_1_, f32[512,128]{1,0:T(8,128)S(1)} %get-tuple-element.23.refs_2_), custom_call_target="tpu_custom_call" | custom-call | flops 600000000 | bytes 1048576 | tf_op jit(solution)/shard_map/pallas_call | solution.py:271
  18.3 3.4 %collective-permute-done.2.q_ref.refs_0_ = bf16[128,256]{1,0:T(8,128)(2,1)S(1)} collective-permute-done((bf16[128,256]{1,0:T(8,128)(2,1)S(1)}, bf16[128,256]{1,0:T(8,128)(2,1)S(1)}, u32[]{:S(2)}, u32[]{:S(2)}) %collective-permute-start.2) | collective-permute-done | bytes 65568 | tf_op jit(solution)/shard_map/ppermute | solution.py:491
  21.8 0.1 collective-permute-done.kv_ref
  21.8 0.6 %shard_map.75.near_ref = bf16[136,256]{1,0:T(8,128)(2,1)S(1)} custom-call(bf16[136,512]{1,0:T(8,128)(2,1)S(1)} %collective-permute-done.kv_ref, bf16[128,256]{1,0:T(8,128)(2,1)S(1)} %get-tuple-element.21.q_ref.refs_0_, f32[128,256]{1,0:T(8,128)S(1)} %get-tuple-element.24.refs_1_, f32[512,128]{1,0:T(8,128)S(1)} %get-tuple-element.25.refs_2_), custom_call_target="tpu_custom_call" | custom-call | flops 600000000 | bytes 1048576 | tf_op jit(solution)/shard_map/pallas_call | solution.py:271
  22.4 0.0 collective-permute-done.8.refs_4_
  22.4 2.8 %collective-permute-start.13 = (bf16[96,2048]{1,0:T(8,128)(2,1)S(1)}, bf16[96,2048]{1,0:T(8,128)(2,1)S(1)}, u32[]{:S(2)}, u32[]{:S(2)}) collective-permute-start(bf16[96,2048]{1,0:T(8,128)(2,1)S(1)} %collective-permute-done.8.refs_4_), channel_id=1, source_target_pairs={{0,1},{1,0},{2,3},{3,2},{4,5},{5,4},{6,7},{7,6},{8,9},{9,8},{10,11... | collective-permute-start | bytes 1179656 | tf_op jit(solution)/shard_map/ppermute | solution.py:465
  25.2 0.6 %shard_map.76 = (f32[128,256]{1,0:T(8,128)S(1)}, f32[512,128]{1,0:T(8,128)S(1)}) custom-call(bf16[128,256]{1,0:T(8,128)(2,1)S(1)} %collective-permute-done.2.q_ref.refs_0_, bf16[136,512]{1,0:T(8,128)(2,1)S(1)} %collective-permute-done.1.kv_ref), custom_call_target="tpu_custom_call" | custom-call | flops 600000000 | bytes 1048576 | tf_op jit(solution)/shard_map/pallas_call | solution.py:271
  25.8 0.6 %shard_map.77 = bf16[128,256]{1,0:T(8,128)(2,1)S(1)} custom-call(bf16[136,512]{1,0:T(8,128)(2,1)S(1)} %collective-permute-done.kv_ref, bf16[128,256]{1,0:T(8,128)(2,1)S(1)} %collective-permute-done.2.q_ref.refs_0_, f32[128,256]{1,0:T(8,128)S(1)} %get-tuple-element.27.refs_1_, f32[512,128]{1,0:T(8,128)S(1)} %get-tuple-element.28.refs_2_), custom_call_target="tpu_custom_call" | custom-call | flops 600000000 | bytes 1048576 | tf_op jit(solution)/shard_map/pallas_call | solution.py:271
  26.4 0.1 collective-permute-start.5
  26.5 0.1 collective-permute-start.11
  26.6 0.0 collective-permute-done.7.refs_3_
  26.6 0.5 %collective-permute-start.12 = (bf16[80,2048]{1,0:T(8,128)(2,1)S(1)}, bf16[80,2048]{1,0:T(8,128)(2,1)S(1)}, u32[]{:S(2)}, u32[]{:S(2)}) collective-permute-start(bf16[80,2048]{1,0:T(8,128)(2,1)S(1)} %collective-permute-done.7.refs_3_), channel_id=1, source_target_pairs={{0,1},{1,0},{2,3},{3,2},{4,5},{5,4},{6,7},{7,6},{8,9},{9,8},{10,11... | collective-permute-start | bytes 983048 | tf_op jit(solution)/shard_map/ppermute | solution.py:465
  27.1 3.9 %collective-permute-done.5.far_x_ref = bf16[128,256]{1,0:T(8,128)(2,1)S(1)} collective-permute-done((bf16[128,256]{1,0:T(8,128)(2,1)S(1)}, bf16[128,256]{1,0:T(8,128)(2,1)S(1)}, u32[]{:S(2)}, u32[]{:S(2)}) %collective-permute-start.5) | collective-permute-done | bytes 65568 | tf_op jit(solution)/shard_map/ppermute | solution.py:526
  31.0 0.3 collective-permute-start.3
  31.3 2.8 %collective-permute-done.3.far_ref = bf16[128,256]{1,0:T(8,128)(2,1)S(1)} collective-permute-done((bf16[128,256]{1,0:T(8,128)(2,1)S(1)}, bf16[128,256]{1,0:T(8,128)(2,1)S(1)}, u32[]{:S(2)}, u32[]{:S(2)}) %collective-permute-start.3) | collective-permute-done | bytes 65568 | tf_op jit(solution)/shard_map/ppermute | solution.py:523
  34.1 1.2 %collective-permute-start.4 = (bf16[136,256]{1,0:T(8,128)(2,1)S(1)}, bf16[136,256]{1,0:T(8,128)(2,1)S(1)}, u32[]{:S(2)}, u32[]{:S(2)}) collective-permute-start(bf16[136,256]{1,0:T(8,128)(2,1)S(1)} %shard_map.75.near_ref), channel_id=1, source_target_pairs={{0,2},{1,3},{2,0},{3,1},{4,6},{5,7},{6,4},{7,5},{8,10},{9,11},{10,... | collective-permute-start | bytes 208904 | tf_op jit(solution)/shard_map/ppermute | solution.py:465
  35.3 1.9 %collective-permute-done.4.near_x_ref = bf16[136,256]{1,0:T(8,128)(2,1)S(1)} collective-permute-done((bf16[136,256]{1,0:T(8,128)(2,1)S(1)}, bf16[136,256]{1,0:T(8,128)(2,1)S(1)}, u32[]{:S(2)}, u32[]{:S(2)}) %collective-permute-start.4) | collective-permute-done | bytes 69664 | tf_op jit(solution)/shard_map/ppermute | solution.py:465
  37.3 3.2 %collective-permute-start.9 = (bf16[128,512]{1,0:T(8,128)(2,1)S(1)}, bf16[128,512]{1,0:T(8,128)(2,1)S(1)}, u32[]{:S(2)}, u32[]{:S(2)}) collective-permute-start(bf16[128,512]{1,0:T(8,128)(2,1)S(1)} %shard_map.78.refs_0_), channel_id=1, source_target_pairs={{0,1},{1,0},{2,3},{3,2},{4,5},{5,4},{6,7},{7,6},{8,9},{9,8},{10,11... | collective-permute-start | bytes 393224 | tf_op jit(solution)/shard_map/ppermute | solution.py:465
  40.5 0.5 %shard_map.79.early_ref = f32[128,2048]{1,0:T(8,128)S(1)} custom-call(bf16[128,512]{1,0:T(8,128)(2,1)S(1)} %shard_map.78.refs_0_, bf16[256,2048]{1,0:T(8,128)(2,1)S(1)} %copy-done, bf16[80,2048]{1,0:T(8,128)(2,1)S(1)} %collective-permute-done.6.refs_2_, bf16[80,2048]{1,0:T(8,128)(2,1)S(1)} %collective-permute-done.7.refs_3_, ...), custom_call_target="tpu_custom_call" | custom-call | flops 268435456 | bytes 1048576 | tf_op jit(solution)/shard_map/pallas_call | solution.py:414
  41.0 0.5 %collective-permute-done.9.refs_0_ = bf16[128,512]{1,0:T(8,128)(2,1)S(1)} collective-permute-done((bf16[128,512]{1,0:T(8,128)(2,1)S(1)}, bf16[128,512]{1,0:T(8,128)(2,1)S(1)}, u32[]{:S(2)}, u32[]{:S(2)}) %collective-permute-start.9) | collective-permute-done | bytes 131104 | tf_op jit(solution)/shard_map/ppermute | solution.py:465
  41.5 0.0 collective-permute-done.11.refs_2_
  41.5 0.0 collective-permute-done.13.refs_4_
  41.5 0.0 collective-permute-done.12.refs_3_
  41.5 0.0 collective-permute-done.10.refs_1_
  41.5 1.1 %shard_map.80 = bf16[128,2048]{1,0:T(8,128)(2,1)} custom-call(f32[128,2048]{1,0:T(8,128)S(1)} %shard_map.79.early_ref, bf16[128,512]{1,0:T(8,128)(2,1)S(1)} %collective-permute-done.9.refs_0_, bf16[256,2048]{1,0:T(8,128)(2,1)S(1)} %collective-permute-done.10.refs_1_, bf16[80,2048]{1,0:T(8,128)(2,1)S(1)} %collective-permute-done.11.refs_2_, ...), custom_call_target="tpu_custom_call" | custom-call | flops 268435456 | bytes 1048576 | tf_op jit(solution)/shard_map/pallas_call | solution.py:414
  (2 shorter events, 0.0 us)
Async XLA Ops:
  2.6 1.2 %copy-start = (bf16[256,2048]{1,0:T(8,128)(2,1)S(1)}, bf16[256,2048]{1,0:T(8,128)(2,1)}, u32[]{:S(2)}) copy-start(bf16[256,2048]{1,0:T(8,128)(2,1)} %refs_1_.1) | copy-start | bytes 3145732
  3.9 37.7 %collective-permute-start.10 = (bf16[256,2048]{1,0:T(8,128)(2,1)S(1)}, bf16[256,2048]{1,0:T(8,128)(2,1)S(1)}, u32[]{:S(2)}, u32[]{:S(2)}) collective-permute-start(bf16[256,2048]{1,0:T(8,128)(2,1)S(1)} %copy-done), channel_id=1, source_target_pairs={{0,1},{1,0},{2,3},{3,2},{4,5},{5,4},{6,7},{7,6},{8,9},{9,8},{10,11... | collective-permute-start | bytes 3145736 | tf_op jit(solution)/shard_map/ppermute | solution.py:465
  4.6 9.3 %collective-permute-start.6 = (bf16[80,2048]{1,0:T(8,128)(2,1)S(1)}, bf16[80,2048]{1,0:T(8,128)(2,1)S(1)}, u32[]{:S(2)}, u32[]{:S(2)}) collective-permute-start(bf16[80,2048]{1,0:T(8,128)(2,1)S(1)} %constant_dynamic-slice_fusion), channel_id=1, source_target_pairs={{0,2},{1,3},{2,0},{3,1},{4,6},{5,7},{6,4},{7,5},{8,10},{9,11},{10,... | collective-permute-start | bytes 983048 | tf_op jit(solution)/shard_map/ppermute | solution.py:465
  5.9 16.6 %collective-permute-start.8 = (bf16[96,2048]{1,0:T(8,128)(2,1)S(1)}, bf16[96,2048]{1,0:T(8,128)(2,1)S(1)}, u32[]{:S(2)}, u32[]{:S(2)}) collective-permute-start(bf16[96,2048]{1,0:T(8,128)(2,1)S(1)} %get-tuple-element.30), channel_id=1, source_target_pairs={{0,2},{1,3},{2,0},{3,1},{4,6},{5,7},{6,4},{7,5},{8,10},{9,11},{10,... | collective-permute-start | bytes 1179656 | tf_op jit(solution)/shard_map/ppermute | solution.py:465
  6.1 10.3 %collective-permute-start.1 = (bf16[136,512]{1,0:T(8,128)(2,1)S(1)}, bf16[136,512]{1,0:T(8,128)(2,1)S(1)}, u32[]{:S(2)}, u32[]{:S(2)}) collective-permute-start(bf16[136,512]{1,0:T(8,128)(2,1)S(1)} %get-tuple-element.20.kv_ref), channel_id=1, source_target_pairs={{0,4},{4,8},{8,12},{12,0},{1,5},{5,9},{9,13},{13,1},{2,6},{6,10},{... | collective-permute-start | bytes 417800 | tf_op jit(solution)/shard_map/ppermute | solution.py:489
  13.9 12.7 %collective-permute-start.7 = (bf16[80,2048]{1,0:T(8,128)(2,1)S(1)}, bf16[80,2048]{1,0:T(8,128)(2,1)S(1)}, u32[]{:S(2)}, u32[]{:S(2)}) collective-permute-start(bf16[80,2048]{1,0:T(8,128)(2,1)S(1)} %collective-permute-done.6.refs_2_), channel_id=1, source_target_pairs={{0,16},{16,0},{1,17},{17,1},{2,18},{18,2},{3,19},{19,3},{4,20},{20... | collective-permute-start | bytes 983048 | tf_op jit(solution)/shard_map/ppermute | solution.py:495
  15.1 6.7 %collective-permute-start = (bf16[136,512]{1,0:T(8,128)(2,1)S(1)}, bf16[136,512]{1,0:T(8,128)(2,1)S(1)}, u32[]{:S(2)}, u32[]{:S(2)}) collective-permute-start(bf16[136,512]{1,0:T(8,128)(2,1)S(1)} %get-tuple-element.20.kv_ref), channel_id=1, source_target_pairs={{0,8},{1,9},{2,10},{3,11},{16,24},{17,25},{18,26},{19,27}} | collective-permute-start | bytes 417800 | tf_op jit(solution)/shard_map/ppermute | solution.py:489
  16.4 5.3 %collective-permute-start.2 = (bf16[128,256]{1,0:T(8,128)(2,1)S(1)}, bf16[128,256]{1,0:T(8,128)(2,1)S(1)}, u32[]{:S(2)}, u32[]{:S(2)}) collective-permute-start(bf16[128,256]{1,0:T(8,128)(2,1)S(1)} %get-tuple-element.21.q_ref.refs_0_), channel_id=1, source_target_pairs={{12,8},{13,9},{14,10},{15,11},{28,24},{29,25},{30,26},{31,27}} | collective-permute-start | bytes 196616 | tf_op jit(solution)/shard_map/ppermute | solution.py:491
  22.4 19.1 %collective-permute-start.13 = (bf16[96,2048]{1,0:T(8,128)(2,1)S(1)}, bf16[96,2048]{1,0:T(8,128)(2,1)S(1)}, u32[]{:S(2)}, u32[]{:S(2)}) collective-permute-start(bf16[96,2048]{1,0:T(8,128)(2,1)S(1)} %collective-permute-done.8.refs_4_), channel_id=1, source_target_pairs={{0,1},{1,0},{2,3},{3,2},{4,5},{5,4},{6,7},{7,6},{8,9},{9,8},{10,11... | collective-permute-start | bytes 1179656 | tf_op jit(solution)/shard_map/ppermute | solution.py:465
  26.4 4.6 %collective-permute-start.5 = (bf16[128,256]{1,0:T(8,128)(2,1)S(1)}, bf16[128,256]{1,0:T(8,128)(2,1)S(1)}, u32[]{:S(2)}, u32[]{:S(2)}) collective-permute-start(bf16[128,256]{1,0:T(8,128)(2,1)S(1)} %shard_map.77), channel_id=1, source_target_pairs={{0,6},{1,7},{2,4},{3,5},{4,2},{5,3},{6,0},{7,1},{8,14},{9,15},{10,... | collective-permute-start | bytes 196616 | tf_op jit(solution)/shard_map/ppermute | solution.py:526
  26.5 15.0 %collective-permute-start.11 = (bf16[80,2048]{1,0:T(8,128)(2,1)S(1)}, bf16[80,2048]{1,0:T(8,128)(2,1)S(1)}, u32[]{:S(2)}, u32[]{:S(2)}) collective-permute-start(bf16[80,2048]{1,0:T(8,128)(2,1)S(1)} %collective-permute-done.6.refs_2_), channel_id=1, source_target_pairs={{0,1},{1,0},{2,3},{3,2},{4,5},{5,4},{6,7},{7,6},{8,9},{9,8},{10,11... | collective-permute-start | bytes 983048 | tf_op jit(solution)/shard_map/ppermute | solution.py:465
  26.6 15.0 %collective-permute-start.12 = (bf16[80,2048]{1,0:T(8,128)(2,1)S(1)}, bf16[80,2048]{1,0:T(8,128)(2,1)S(1)}, u32[]{:S(2)}, u32[]{:S(2)}) collective-permute-start(bf16[80,2048]{1,0:T(8,128)(2,1)S(1)} %collective-permute-done.7.refs_3_), channel_id=1, source_target_pairs={{0,1},{1,0},{2,3},{3,2},{4,5},{5,4},{6,7},{7,6},{8,9},{9,8},{10,11... | collective-permute-start | bytes 983048 | tf_op jit(solution)/shard_map/ppermute | solution.py:465
  31.0 3.1 %collective-permute-start.3 = (bf16[128,256]{1,0:T(8,128)(2,1)S(1)}, bf16[128,256]{1,0:T(8,128)(2,1)S(1)}, u32[]{:S(2)}, u32[]{:S(2)}) collective-permute-start(bf16[128,256]{1,0:T(8,128)(2,1)S(1)} %shard_map.77), channel_id=1, source_target_pairs={{0,4},{4,0},{8,12},{12,8},{1,5},{5,1},{9,13},{13,9},{2,6},{6,2},{1... | collective-permute-start | bytes 196616 | tf_op jit(solution)/shard_map/ppermute | solution.py:523
  34.1 3.2 %collective-permute-start.4 = (bf16[136,256]{1,0:T(8,128)(2,1)S(1)}, bf16[136,256]{1,0:T(8,128)(2,1)S(1)}, u32[]{:S(2)}, u32[]{:S(2)}) collective-permute-start(bf16[136,256]{1,0:T(8,128)(2,1)S(1)} %shard_map.75.near_ref), channel_id=1, source_target_pairs={{0,2},{1,3},{2,0},{3,1},{4,6},{5,7},{6,4},{7,5},{8,10},{9,11},{10,... | collective-permute-start | bytes 208904 | tf_op jit(solution)/shard_map/ppermute | solution.py:465
  37.3 4.2 %collective-permute-start.9 = (bf16[128,512]{1,0:T(8,128)(2,1)S(1)}, bf16[128,512]{1,0:T(8,128)(2,1)S(1)}, u32[]{:S(2)}, u32[]{:S(2)}) collective-permute-start(bf16[128,512]{1,0:T(8,128)(2,1)S(1)} %shard_map.78.refs_0_), channel_id=1, source_target_pairs={{0,1},{1,0},{2,3},{3,2},{4,5},{5,4},{6,7},{7,6},{8,9},{9,8},{10,11... | collective-permute-start | bytes 393224 | tf_op jit(solution)/shard_map/ppermute | solution.py:465
